TPU v7x, 32 devices: a whole 2x2x4 slice. The times are simulated.
32 devices in a mesh: sp: 8 (over z, x), tp: 4 (over y, core).
Axes of the slice: x: 2, y: 2, z: 4, core: 2. Of those that a mesh axis runs over, the one named last changes fastest.
Arguments:
- resid: bfloat16 [2048, 4096], P('sp'), may hold values from -6 to 6
- queries: bfloat16 [2048, 3072], P('sp', 'tp'), may hold values from -1000 to 1000
- latent: bfloat16 [2048, 512], P('sp'), may hold values from -6 to 6
- rope_key: bfloat16 [2048, 64], P('sp'), may hold values from -6 to 6
- lat_gain: float32 [512], replicated, may hold values from 0.1 to 1.9
- kv_weight: bfloat16 [512, 4096], P(None, 'tp'), may hold values from -4 to 4
- out_gain: float32 [2048], P('tp'), may hold values from 0.1 to 1.9
- out_weight: bfloat16 [2048, 4096], P('tp'), may hold values from -0.125 to 0.125
- ffn_gain: float32 [4096], replicated, may hold values from 0.1 to 1.9
- gate_weight: bfloat16 [4096, 6144], P('sp', 'tp'), may hold values from -0.09375 to 0.09375
- up_weight: bfloat16 [4096, 6144], P('sp', 'tp'), may hold values from -0.09375 to 0.09375
- down_weight: bfloat16 [6144, 4096], P('tp', 'sp'), may hold values from -0.078125 to 0.078125
Outputs:
- result: bfloat16 [2048, 4096], P(('sp', 'tp'))
All inputs are finite; a program needn't handle non-finite values.
Results may differ from a plain program's by a relative error of at most 0.018.
Values may be sent and summed in bfloat16 or wider, within the bound.
A program may use at most 192 MiB of HBM per device.

v0:
```python
import math

import jax
import jax.numpy as jnp
from jax import lax
from jax.experimental import pallas as pl
from jax.experimental.pallas import tpu as pltpu
from jax.sharding import PartitionSpec as P


HEADS = 16
NOPE = 128
ROPE = 64
VDIM = 128


EPSILON = 1e-06
THETA = 10000.0
LOWEST = -1e30
GROUP = 4


def rotate(values, places):
    half = values.shape[-1] // 2
    inverse = THETA ** (-jnp.arange(half, dtype=jnp.float32) / half)
    angle = places[..., None] * inverse
    cosine = jnp.cos(angle)
    sine = jnp.sin(angle)
    first = values[..., :half]
    second = values[..., half:]
    return jnp.concatenate(
        [first * cosine - second * sine, first * sine + second * cosine], axis=-1
    )


def norm_rows(values, gain):
    wide = values.astype(jnp.float32)
    return wide * lax.rsqrt(jnp.mean(wide * wide, axis=-1, keepdims=True) + EPSILON) * gain


def make_keys(latent_piece, rotary_piece, lat_gain, kv_weight, key_index):
    normed = norm_rows(latent_piece, lat_gain).astype(jnp.bfloat16)
    key_value = jnp.dot(normed, kv_weight, preferred_element_type=jnp.float32)
    key_value = key_value.astype(jnp.bfloat16)
    key_rope = rotate(rotary_piece.astype(jnp.float32), key_index.astype(jnp.float32)).astype(
        jnp.bfloat16
    )
    return (key_value, key_rope)


def to_near(values, flip):
    ranks = lax.axis_size("sp")
    return lax.ppermute(values, "sp", [(rank, rank ^ flip) for rank in range(ranks)])


def to_high(values, step, ranks):
    if step % (ranks // GROUP) == 0:
        return values
    return lax.ppermute(
        values, "sp", [(rank, (rank + step * GROUP) % ranks) for rank in range(ranks)]
    )


def reorder(blocks, place):
    bit = 1
    while bit < len(blocks):
        swap = place // bit % 2 == 1
        blocks = [jnp.where(swap, blocks[j ^ bit], blocks[j]) for j in range(len(blocks))]
        bit *= 2
    return blocks


def by_distance(values, place):
    return jnp.concatenate(reorder(jnp.split(values, GROUP, axis=1), place), axis=1)


def to_column(values, bit):
    columns = lax.axis_size("tp")
    return lax.ppermute(values, "tp", [(column, column ^ bit) for column in range(columns)])


def gather_columns(values):
    rows = values.shape[0]
    held = {0: values}
    bit = lax.axis_size("tp") // 2
    while bit:
        keys = sorted(held)
        theirs = to_column(jnp.concatenate([held[key] for key in keys], axis=0), bit)
        for at, key in enumerate(keys):
            held[key + bit] = theirs[at * rows : (at + 1) * rows]
        bit //= 2
    return jnp.concatenate([held[key] for key in sorted(held)], axis=0)


def scatter_columns(values):
    columns = lax.axis_size("tp")
    blocks = dict(enumerate(jnp.split(values, columns, axis=0)))
    bit = 1
    while bit < columns:
        mine = [key for key in sorted(blocks) if not key & bit]
        theirs = to_column(jnp.concatenate([blocks[key + bit] for key in mine], axis=0), bit)
        theirs = jnp.split(theirs, len(mine), axis=0)
        blocks = {
            key: (blocks[key].astype(jnp.float32) + piece.astype(jnp.float32)).astype(jnp.bfloat16)
            for key, piece in zip(mine, theirs)
        }
        bit *= 2
    return blocks[0]


def near_weights(gate, up, down):
    gate_one = to_near(gate, 1)
    up_two = to_near(up, 2)
    up_one = to_near(up, 1)
    gate_two = to_near(gate, 2)
    gate_both = to_near(gate_one, 2)
    up_both = to_near(up_two, 1)
    down, gate_both, up_both = lax.optimization_barrier((down, gate_both, up_both))
    half = down.shape[0] // 2
    down_one = to_near(down, 1)
    down_two = to_near(down, 2)
    far = [to_near(down_one[:half], 2), to_near(down_two[half:], 1)]
    down_both = jnp.concatenate(far, axis=0)
    return (
        (gate, gate_one, gate_two, gate_both),
        (up, up_one, up_two, up_both),
        (down, down_one, down_two, down_both),
    )


def blocks_dot(rows, weights, block):
    return sum(
        jnp.dot(
            rows[:, place * block : (place + 1) * block], weight, preferred_element_type=jnp.float32
        )
        for place, weight in enumerate(weights)
    )


def plain_body(
    resid,
    queries,
    latent,
    rope_key,
    lat_gain,
    kv_weight,
    out_gain,
    out_weight,
    ffn_gain,
    gate_weight,
    up_weight,
    down_weight,
):
    gate_blocks, up_blocks, down_blocks = near_weights(gate_weight, up_weight, down_weight)
    rows_here = resid.shape[0]
    first_row = lax.axis_index("sp") * rows_here
    heads_here = queries.shape[1] // (NOPE + ROPE)
    columns = lax.axis_size("tp")
    column = lax.axis_index("tp")
    share = rows_here // columns
    query = jnp.concatenate(reorder(jnp.split(queries, columns, axis=0), column), axis=0)
    query = query.reshape(rows_here, heads_here, NOPE + ROPE)
    within = jnp.arange(rows_here, dtype=jnp.int32)
    own_columns = (within // share) ^ column
    query_index = first_row + own_columns * share + within % share
    query_nope = query[:, :, :NOPE]
    query_rope = rotate(
        query[:, :, NOPE:].astype(jnp.float32), query_index.astype(jnp.float32)[:, None]
    ).astype(jnp.bfloat16)
    scale = 1.0 / math.sqrt(NOPE + ROPE)

    def accumulate(state, key_value, key_rope):
        running_max, running_sum, weighted = state
        length = key_value.shape[0]
        key_value = key_value.reshape(length, heads_here, NOPE + VDIM)
        scores = jnp.einsum(
            "qhd,khd->hqk", query_nope, key_value[:, :, :NOPE], preferred_element_type=jnp.float32
        )
        scores = (
            scores
            + jnp.einsum("qhr,kr->hqk", query_rope, key_rope, preferred_element_type=jnp.float32)
        ) * scale
        allowed = (key_index[None, :] <= query_index[:, None])[None]
        scores = jnp.where(allowed, scores, LOWEST)
        new_max = jnp.maximum(running_max, jnp.max(scores, axis=-1))
        weights = jnp.where(allowed, jnp.exp(scores - new_max[:, :, None]), 0.0)
        running_sum = jnp.sum(weights, axis=-1)
        added = jnp.einsum(
            "hqk,khd->qhd",
            weights.astype(jnp.bfloat16),
            key_value[:, :, NOPE:],
            preferred_element_type=jnp.float32,
        )
        weighted = added
        return (new_max, running_sum, weighted)

    initial = (
        jnp.full((heads_here, rows_here), LOWEST, jnp.float32),
        jnp.zeros((heads_here, rows_here), jnp.float32),
        jnp.zeros((rows_here, heads_here, VDIM), jnp.float32),
    )
    ranks = lax.axis_size("sp")
    rank = lax.axis_index("sp")
    both = jnp.concatenate([latent, rope_key], axis=1)
    both = lax.dynamic_slice_in_dim(both, column * share, share, 0)
    pieces = [both]
    for step in range(1, ranks):
        onward = [(source, source + step) for source in range(ranks - step)]
        pieces.append(lax.ppermute(both, "sp", onward))
    both = gather_columns(jnp.concatenate(pieces, axis=0))
    within = jnp.arange(both.shape[0], dtype=jnp.int32)
    source = (rank - within // share % ranks + ranks) % ranks
    key_index = source * rows_here + ((within // (share * ranks)) ^ column) * share + within % share
    pieces = (both[:, : latent.shape[1]], both[:, latent.shape[1] :])

    def update(state):
        key_value, key_rope = make_keys(pieces[0], pieces[1], lat_gain, kv_weight, key_index)
        return accumulate(state, key_value, key_rope)

    _, running_sum, weighted = update(initial)
    attended = (weighted / jnp.transpose(running_sum)[:, :, None]).astype(jnp.bfloat16)
    attended_float = attended.reshape(rows_here, heads_here * VDIM).astype(jnp.float32)
    squares = jnp.split(jnp.sum(attended_float * attended_float, axis=1), columns)
    squares = lax.psum(jnp.concatenate(reorder(squares, column)), "tp")
    squares = jnp.concatenate(reorder(jnp.split(squares, columns), column))
    normed_out = attended_float * lax.rsqrt(squares / (HEADS * VDIM) + EPSILON)[:, None] * out_gain
    normed_out = normed_out.astype(jnp.bfloat16)
    own_first = lax.axis_index("tp") * share
    projected = jnp.dot(normed_out, out_weight, preferred_element_type=jnp.float32)
    projected = projected.astype(jnp.bfloat16)
    attn_sum = scatter_columns(projected).astype(jnp.float32)
    own_resid = lax.dynamic_slice_in_dim(resid, own_first, share, 0)
    middle = (own_resid.astype(jnp.float32) + attn_sum).astype(jnp.bfloat16)
    highs = ranks // GROUP
    high = rank // GROUP
    place = rank % GROUP
    width = resid.shape[1]
    block = width // ranks
    wide = GROUP * block
    mids = norm_rows(middle, ffn_gain).astype(jnp.bfloat16)
    mids = [
        to_high(
            by_distance(
                lax.dynamic_slice_in_dim(mids, (high + step) % highs * wide, wide, 1), place
            ),
            step,
            ranks,
        )
        for step in range(highs)
    ]
    mids = [gather_columns(piece) for piece in mids]
    gates, ups = None, None
    for step in list(range(1, highs)) + [0]:
        piece = mids[step]
        gate = blocks_dot(piece, gate_blocks, block)
        up = blocks_dot(piece, up_blocks, block)
        if step:
            gate = to_high(gate.astype(jnp.bfloat16), highs - step, ranks).astype(jnp.float32)
            up = to_high(up.astype(jnp.bfloat16), highs - step, ranks).astype(jnp.float32)
        gates = gate if gates is None else gates + gate
        ups = up if ups is None else ups + up
    hidden = (jax.nn.silu(gates) * ups).astype(jnp.bfloat16)
    received = [to_high(hidden, step, ranks) for step in range(highs)]
    terms = []
    for step in range(highs):
        partial = jnp.concatenate(
            [
                jnp.dot(received[step], weight, preferred_element_type=jnp.float32).astype(
                    jnp.bfloat16
                )
                for weight in down_blocks
            ],
            axis=1,
        )
        partial = to_high(scatter_columns(partial), highs - step, ranks)
        terms.append(by_distance(partial, place))
    terms = jnp.concatenate(terms, axis=1)
    ffn_sum = jnp.concatenate(
        [
            lax.dynamic_slice_in_dim(terms, (index - high + highs) % highs * wide, wide, 1)
            for index in range(highs)
        ],
        axis=1,
    ).astype(jnp.float32)
    return (middle.astype(jnp.float32) + ffn_sum).astype(jnp.bfloat16)


LANES = 128
PAIR = 2
LINE = 4
COLUMNS = 4
MESH = pl.DeviceIdType.MESH


def whole_step(
    lat_ref,
    query_ref,
    resid_ref,
    out_gain_ref,
    ffn_gain_ref,
    kv_hbm,
    out_hbm,
    gate_hbm,
    up_hbm,
    down_hbm,
    result_ref,
    lat_buf,
    kv_w,
    out_w,
    gate_up,
    down,
    act,
    hidden,
    top,
    norm,
    acc,
    stats_mine,
    stats_in,
    partial,
    core_in,
    near_out,
    near_in,
    line_out,
    line_in,
    middle,
    total,
    local_sem,
    lat_send,
    lat_recv,
    lat_spread_send,
    lat_spread_recv,
    turn_send,
    turn_recv,
    pair_send,
    pair_recv,
    act_line_send,
    act_line_recv,
    act_spread_send,
    act_spread_recv,
    stat_send,
    stat_recv,
    core_send,
    core_recv,
    near_send,
    near_recv,
    line_send,
    line_recv,
):
    rank = lax.axis_index("sp")
    col = lax.axis_index("tp")
    ranks = lat_buf.shape[0]
    rows = lat_buf.shape[1]
    share = lat_ref.shape[0]
    width = resid_ref.shape[1]
    units = hidden.shape[1]
    block = gate_hbm.shape[0]
    latent = kv_w.shape[0]
    heads = query_ref.shape[1] // (2 * LANES)
    z = rank // PAIR
    x = rank % PAIR
    mate = z * PAIR + (PAIR - 1 - x)
    inner = ((z + 1) // 2) % 2
    z_flips = [z, z + 1 - 2 * (z % 2), (z + 2) % LINE, LINE - 1 - z]
    col_flips = [col, col + 1 - 2 * (col % 2), (col + 2) % COLUMNS, COLUMNS - 1 - col]
    pending = []

    def remote(src, dst, send, recv, sp=None, tp=None):
        target = (rank if sp is None else sp, col if tp is None else tp)
        return pltpu.make_async_remote_copy(
            src_ref=src, dst_ref=dst, send_sem=send, recv_sem=recv, device_id=target,
            device_id_type=MESH,
        )

    def arrived(dst, recv):
        remote(dst, dst, recv, recv, tp=col_flips[1]).wait_recv()

    def send(copy, when=None):
        if when is None:
            copy.start()
        else:
            pl.when(when)(copy.start)
        pending.append((copy, when))

    barrier = pltpu.get_barrier_semaphore()
    for step in range(1, ranks):
        pl.semaphore_signal(
            barrier, inc=1, device_id=((rank + step) % ranks, col), device_id_type=MESH
        )
    for flip in col_flips[1:]:
        pl.semaphore_signal(barrier, inc=1, device_id=(rank, flip), device_id_type=MESH)
    pl.semaphore_wait(barrier, ranks - 1 + COLUMNS - 1)

    def lat_piece(source, column):
        return lat_buf.at[source, pl.ds(pl.multiple_of(column * share, share), share), :]

    def lat_spread(source, piece, flip, slot):
        return remote(
            piece, lat_piece(source, col_flips[slot - flip]),
            lat_spread_send.at[source, slot - 1], lat_spread_recv.at[source, slot - 1],
            tp=col_flips[flip],
        )

    for step in range(1, ranks):
        send(
            remote(
                lat_ref, lat_piece(rank, col), lat_send.at[step - 1], lat_recv.at[rank],
                sp=(rank + step) % ranks,
            ),
            rank + step < ranks,
        )
    lat_spread(rank, lat_ref, 2, 2).start()
    lat_spread(rank, lat_ref, 1, 1).start()
    lat_buf[rank, pl.ds(pl.multiple_of(col * share, share), share), :] = lat_ref[...]

    def region(kind, source):
        at = pl.multiple_of(source * block, block)
        if kind == 2:
            return down.at[:, pl.ds(at, block)]
        return gate_up.at[pl.ds(at, block), pl.ds(kind * units, units)]

    def own_part(kind, place):
        at = pl.multiple_of(place * units, units)
        if kind == 2:
            return down_hbm.at[pl.ds(at, units), :]
        return (gate_hbm, up_hbm)[kind].at[:, pl.ds(at, units)]

    def local(src, dst, slot):
        copy = pltpu.make_async_copy(src, dst, local_sem.at[slot])
        copy.start()
        return copy

    kv_copy = local(kv_hbm, kv_w, 0)
    out_copy = local(out_hbm, out_w, 1)
    own_copies = [local(own_part(kind, z), region(kind, rank), 2 + kind) for kind in range(3)]

    def turn(kind):
        for k in range(1, LINE):
            send(
                remote(
                    own_part(kind, z_flips[k]), region(kind, rank), turn_send.at[kind, k],
                    turn_recv.at[kind, k], sp=z_flips[k] * PAIR + x,
                )
            )

    def pump(kind, k):
        here = region(kind, z_flips[k] * PAIR + x)
        if k:
            arrived(here, turn_recv.at[kind, k])
        send(
            remote(
                here if k else own_part(kind, z), here, pair_send.at[kind, k],
                pair_recv.at[kind, k], sp=mate,
            )
        )

    def paired(kind):
        for k in range(LINE):
            arrived(region(kind, z_flips[k] * PAIR + (PAIR - 1 - x)), pair_recv.at[kind, k])

    turn(0)
    turn(1)
    pump(0, 0)
    pump(1, 0)

    top[...] = jnp.full(top.shape, LOWEST, jnp.float32)
    norm[...] = jnp.zeros(norm.shape, jnp.float32)
    acc[...] = jnp.zeros(acc.shape, jnp.float32)
    scale = 1.0 / math.sqrt(NOPE + ROPE)
    kv_copy.wait()

    def attend(index, carry):
        source = rank - index

        @pl.when(index < rank)
        def _():
            arrived(lat_piece(source - 1, col), lat_recv.at[source - 1])
            piece = lat_piece(source - 1, col)
            lat_spread(source - 1, piece, 2, 2).start()
            lat_spread(source - 1, piece, 1, 1).start()

        arrived(lat_piece(source, col_flips[2]), lat_spread_recv.at[source, 1])
        lat_spread(source, lat_piece(source, col_flips[2]), 1, 3).start()
        arrived(lat_piece(source, col_flips[1]), lat_spread_recv.at[source, 0])
        arrived(lat_piece(source, col_flips[3]), lat_spread_recv.at[source, 2])
        key_value = jnp.dot(
            lat_buf[source, :, :latent], kv_w[...], preferred_element_type=jnp.float32
        ).astype(jnp.bfloat16)
        key_rope = lat_buf[source, :, latent:]
        row_of = lax.broadcasted_iota(jnp.int32, (rows, rows), 0) + index * rows
        allowed = lax.broadcasted_iota(jnp.int32, (rows, rows), 1) <= row_of
        for head in range(heads):
            at = head * (NOPE + VDIM)
            keys = jnp.concatenate([key_value[:, at : at + NOPE], key_rope], axis=1)
            scores = lax.dot_general(
                query_ref[:, head * 2 * LANES : (head + 1) * 2 * LANES], keys,
                (((1,), (1,)), ((), ())), preferred_element_type=jnp.float32,
            )
            scores = jnp.where(allowed, scores * scale, LOWEST)
            old = top[head]
            new = jnp.maximum(old, jnp.max(scores, axis=1, keepdims=True))
            weights = jnp.exp(scores - new[:, :1])
            fade = jnp.exp(old - new)
            top[head] = new
            norm[head] = norm[head] * fade + jnp.sum(weights, axis=1, keepdims=True)
            across = slice(head * VDIM, (head + 1) * VDIM)
            acc[:, across] = acc[:, across] * fade + jnp.dot(
                weights.astype(jnp.bfloat16), key_value[:, at + NOPE : at + NOPE + VDIM],
                preferred_element_type=jnp.float32,
            )
        return carry

    lax.fori_loop(0, rank + 1, attend, 0)
    for kind, k in ((0, 1), (1, 1), (0, 2)):
        pump(kind, k)

    squares = jnp.zeros((rows, 1), jnp.float32)
    attended = []
    for head in range(heads):
        across = slice(head * VDIM, (head + 1) * VDIM)
        part = (acc[:, across] / norm[head]).astype(jnp.bfloat16).astype(jnp.float32)
        squares = squares + jnp.sum(part * part, axis=1, keepdims=True)
        attended.append((part * out_gain_ref[:, across]).astype(jnp.bfloat16))
    attended = jnp.concatenate(attended, axis=1)
    stats_mine[...] = jnp.broadcast_to(squares, stats_mine.shape)

    chunk = 4 * LANES
    chunks = width // chunk

    def piece_of(ref, slot, column):
        return ref.at[slot, pl.ds(pl.multiple_of(column * share, share), share), :]

    def project(slot, left, right):
        def one(index, carry):
            at = pl.ds(pl.multiple_of(index * chunk, chunk), chunk)
            partial[slot, :, at] = jnp.dot(
                left, right[:, at], preferred_element_type=jnp.float32
            ).astype(jnp.bfloat16)
            return carry

        lax.fori_loop(0, chunks, one, 0)

    def each_chunk(work):
        def one(index, carry):
            work(pl.ds(pl.multiple_of(index * chunk, chunk), chunk))
            return carry

        lax.fori_loop(0, chunks, one, 0)

    def fold(slot):
        send(
            remote(
                piece_of(partial, slot, col_flips[3]), core_in.at[slot, 1],
                core_send.at[slot, 1], core_recv.at[slot, 1], tp=col_flips[1],
            )
        )
        send(
            remote(
                piece_of(partial, slot, col_flips[1]), core_in.at[slot, 0],
                core_send.at[slot, 0], core_recv.at[slot, 0], tp=col_flips[1],
            )
        )
        arrived(core_in.at[slot, 1], core_recv.at[slot, 1])

        def add(at):
            theirs = partial[
                slot, pl.ds(pl.multiple_of(col_flips[2] * share, share), share), at
            ].astype(jnp.float32)
            near_out[slot, :, at] = (theirs + core_in[slot, 1, :, at].astype(jnp.float32)).astype(
                jnp.bfloat16
            )

        each_chunk(add)
        send(
            remote(
                near_out.at[slot], near_in.at[slot], near_send.at[slot], near_recv.at[slot],
                tp=col_flips[2],
            )
        )
        arrived(core_in.at[slot, 0], core_recv.at[slot, 0])

    def folded(slot):
        arrived(near_in.at[slot], near_recv.at[slot])

        def add(at):
            mine = partial[slot, pl.ds(pl.multiple_of(col * share, share), share), at]
            total[:, at] = (
                mine.astype(jnp.float32)
                + core_in[slot, 0, :, at].astype(jnp.float32)
                + near_in[slot, :, at].astype(jnp.float32)
            )

        each_chunk(add)

    out_copy.wait()
    first = LINE
    for m in range(1, COLUMNS):
        send(
            remote(
                stats_mine.at[pl.ds(pl.multiple_of(col_flips[m] * share, share), share), :],
                stats_in.at[m - 1], stat_send.at[m - 1], stat_recv.at[m - 1], tp=col_flips[m],
            )
        )
    project(first, attended, out_w)
    fold(first)
    for kind, k in ((1, 2), (0, 3)):
        pump(kind, k)
    squares = stats_mine[pl.ds(pl.multiple_of(col * share, share), share), :]
    for m in range(1, COLUMNS):
        arrived(stats_in.at[m - 1], stat_recv.at[m - 1])
        squares = squares + stats_in[m - 1]
    factor = lax.rsqrt(squares / (HEADS * VDIM) + EPSILON)[:, :1]
    folded(first)
    squares = jnp.zeros((share, 1), jnp.float32)
    for index in range(chunks):
        at = slice(index * chunk, (index + 1) * chunk)
        mid = (resid_ref[:, at].astype(jnp.float32) + total[:, at] * factor).astype(jnp.bfloat16)
        middle[:, at] = mid
        mid = mid.astype(jnp.float32)
        squares = squares + jnp.sum(mid * mid, axis=1, keepdims=True)
    factor = lax.rsqrt(squares / width + EPSILON)

    def act_piece(place, column):
        at = pl.multiple_of(place * rows + column * share, share)
        return act.at[pl.ds(at, share), :]

    own_rows = pl.ds(pl.multiple_of(z * rows + col * share, share), share)
    for index in range(chunks):
        at = slice(index * chunk, (index + 1) * chunk)
        act[own_rows, at] = (
            middle[:, at].astype(jnp.float32) * factor * ffn_gain_ref[:, at]
        ).astype(jnp.bfloat16)

    def up_line(src, dst, send_sem, recv_sem, when):
        send(remote(src, dst, send_sem, recv_sem, sp=(rank + PAIR) % ranks), when)

    def down_line(src, dst, send_sem, recv_sem, when):
        send(remote(src, dst, send_sem, recv_sem, sp=(rank + ranks - PAIR) % ranks), when)

    def act_spread(place, index, flip, slot):
        piece = act_piece(place, col_flips[slot - flip])
        send(
            remote(
                piece, piece, act_spread_send.at[index, slot - 1],
                act_spread_recv.at[index, slot - 1], tp=col_flips[flip],
            )
        )

    mine = act_piece(z, col)
    up_line(mine, mine, act_line_send.at[0], act_line_recv.at[z], z < LINE - 1)
    down_line(mine, mine, act_line_send.at[1], act_line_recv.at[z], z > 0)
    act_spread(z, 0, 2, 2)
    act_spread(z, 0, 1, 1)
    pump(1, 3)
    order = [
        z,
        z_flips[1],
        z_flips[2] * (1 - inner) + z_flips[3] * inner,
        z_flips[3] * (1 - inner) + z_flips[2] * inner,
    ]
    for index in range(LINE):
        place = order[index]
        if index < LINE - 1:
            nearer = order[index + 1]
            piece = act_piece(nearer, col)
            arrived(piece, act_line_recv.at[nearer])
            up_line(
                piece, piece, act_line_send.at[2 + 2 * index], act_line_recv.at[nearer],
                (nearer < z) & (z < LINE - 1),
            )
            down_line(
                piece, piece, act_line_send.at[3 + 2 * index], act_line_recv.at[nearer],
                (nearer > z) & (z > 0),
            )
            act_spread(nearer, index + 1, 2, 2)
            act_spread(nearer, index + 1, 1, 1)
        if index == LINE - 2:
            turn(2)
            pump(2, 0)
        if index == 0:
            own_copies[0].wait()
            own_copies[1].wait()
            paired(0)
            paired(1)
        arrived(act_piece(place, col_flips[2]), act_spread_recv.at[index, 1])
        act_spread(place, index, 1, 3)
        arrived(act_piece(place, col_flips[1]), act_spread_recv.at[index, 0])
        arrived(act_piece(place, col_flips[3]), act_spread_recv.at[index, 2])
        here = pl.ds(pl.multiple_of(place * rows, rows), rows)
        both = jnp.dot(act[here, :], gate_up[...], preferred_element_type=jnp.float32)
        gate = both[:, :units]
        hidden[here, :] = (gate / (1.0 + jnp.exp(-gate)) * both[:, units:]).astype(jnp.bfloat16)

    for k in range(1, LINE):
        pump(2, k)
    own_copies[2].wait()
    paired(2)

    def start_rows(slot):
        place = z_flips[LINE - 1 - slot]
        left = hidden[pl.ds(pl.multiple_of(place * rows, rows), rows), :]
        project(slot, left, down)
        fold(slot)

    def add_line(slot):
        def add(at):
            total[:, at] = total[:, at] + line_in[slot, :, at].astype(jnp.float32)

        each_chunk(add)

    def pass_rows(slot):
        place = z_flips[LINE - 1 - slot]
        folded(slot)

        @pl.when(((place > z) & (z > 0)) | ((place < z) & (z < LINE - 1)))
        def _():
            arrived(line_in.at[place], line_recv.at[place])
            add_line(place)

        def keep(at):
            line_out[slot, :, at] = total[:, at].astype(jnp.bfloat16)

        each_chunk(keep)
        up_line(
            line_out.at[slot], line_in.at[place], line_send.at[slot, 0], line_recv.at[place],
            place > z,
        )
        last = jnp.where(place == z - 1, LINE, place)
        down_line(
            line_out.at[slot], line_in.at[last], line_send.at[slot, 1], line_recv.at[last],
            place < z,
        )

    start_rows(0)
    start_rows(1)
    pass_rows(0)
    start_rows(2)
    pass_rows(1)
    start_rows(3)
    pass_rows(2)
    folded(LINE - 1)

    @pl.when(z > 0)
    def _():
        arrived(line_in.at[z], line_recv.at[z])
        add_line(z)

    @pl.when(z < LINE - 1)
    def _():
        arrived(line_in.at[LINE], line_recv.at[LINE])
        add_line(LINE)

    def finish(at):
        result_ref[:, at] = (middle[:, at].astype(jnp.float32) + total[:, at]).astype(jnp.bfloat16)

    each_chunk(finish)

    for copy, when in pending:
        if when is None:
            copy.wait_send()
        else:
            pl.when(when)(copy.wait_send)

    def drain(source, carry):
        piece = lat_piece(source, col)
        for slot in range(COLUMNS - 1):
            remote(
                piece, piece, lat_spread_send.at[source, slot], lat_spread_send.at[source, slot],
                tp=col_flips[1],
            ).wait_send()
        return carry

    lax.fori_loop(0, rank + 1, drain, 0)


def fused_body(
    resid,
    queries,
    latent,
    rope_key,
    lat_gain,
    kv_weight,
    out_gain,
    out_weight,
    ffn_gain,
    gate_weight,
    up_weight,
    down_weight,
):
    ranks, columns = lax.axis_size("sp"), lax.axis_size("tp")
    rank, column = lax.axis_index("sp"), lax.axis_index("tp")
    rows, width = resid.shape
    share = rows // columns
    heads = queries.shape[1] // (NOPE + ROPE)
    units = gate_weight.shape[1] // LINE
    block = gate_weight.shape[0]
    own_first = column * share
    first_row = rank * rows

    def mine(values):
        return lax.dynamic_slice_in_dim(values, own_first, share, 0)

    places = (first_row + jnp.arange(rows, dtype=jnp.int32)).astype(jnp.float32)
    normed = norm_rows(mine(latent), lat_gain).astype(jnp.bfloat16)
    key_rope = rotate(mine(rope_key).astype(jnp.float32), mine(places)).astype(jnp.bfloat16)
    message = jnp.concatenate([normed, key_rope, jnp.zeros_like(key_rope)], axis=1)
    query = queries.reshape(rows, heads, NOPE + ROPE)
    query_rope = rotate(query[:, :, NOPE:].astype(jnp.float32), places[:, None]).astype(
        jnp.bfloat16
    )
    query = jnp.concatenate([query[:, :, :NOPE], query_rope, jnp.zeros_like(query_rope)], axis=2)
    query = query.reshape(rows, heads * 2 * LANES)
    bf, f32 = jnp.bfloat16, jnp.float32
    dma = pltpu.SemaphoreType.DMA
    slots = LINE + 1
    vmem = pl.BlockSpec(memory_space=pltpu.VMEM)
    anywhere = pl.BlockSpec(memory_space=pl.ANY)
    return pl.pallas_call(
        whole_step,
        out_shape=jax.ShapeDtypeStruct((share, width), bf),
        in_specs=[vmem] * 5 + [anywhere] * 5,
        out_specs=vmem,
        scratch_shapes=[
            pltpu.VMEM((ranks, rows, message.shape[1]), bf),
            pltpu.VMEM(kv_weight.shape, bf),
            pltpu.VMEM(out_weight.shape, bf),
            pltpu.VMEM((ranks * block, 2 * units), bf),
            pltpu.VMEM((units, ranks * down_weight.shape[1]), bf),
            pltpu.VMEM((LINE * rows, width), bf),
            pltpu.VMEM((LINE * rows, units), bf),
            pltpu.VMEM((heads, rows, LANES), f32),
            pltpu.VMEM((heads, rows, LANES), f32),
            pltpu.VMEM((rows, heads * VDIM), f32),
            pltpu.VMEM((rows, LANES), f32),
            pltpu.VMEM((columns - 1, share, LANES), f32),
            pltpu.VMEM((slots, rows, width), bf),
            pltpu.VMEM((slots, 2, share, width), bf),
            pltpu.VMEM((slots, share, width), bf),
            pltpu.VMEM((slots, share, width), bf),
            pltpu.VMEM((LINE, share, width), bf),
            pltpu.VMEM((slots, share, width), bf),
            pltpu.VMEM((share, width), bf),
            pltpu.VMEM((share, width), f32),
            dma((5,)),
            dma((ranks - 1,)),
            dma((ranks,)),
            dma((ranks, columns - 1)),
            dma((ranks, columns - 1)),
            dma((3, LINE)),
            dma((3, LINE)),
            dma((3, LINE)),
            dma((3, LINE)),
            dma((2 * LINE,)),
            dma((LINE,)),
            dma((LINE, columns - 1)),
            dma((LINE, columns - 1)),
            dma((columns - 1,)),
            dma((columns - 1,)),
            dma((slots, 2)),
            dma((slots, 2)),
            dma((slots,)),
            dma((slots,)),
            dma((LINE, 2)),
            dma((slots,)),
        ],
        compiler_params=pltpu.CompilerParams(
            collective_id=0, has_side_effects=True, vmem_limit_bytes=66 * 1024 * 1000
        ),
    )(
        message,
        query,
        mine(resid),
        out_gain.reshape(1, -1),
        ffn_gain.reshape(1, -1),
        kv_weight,
        out_weight,
        gate_weight,
        up_weight,
        down_weight,
    )


def solution(mesh):
    placed = (
        P("sp", None),
        P("sp", "tp"),
        P("sp", None),
        P("sp", None),
        P(),
        P(None, "tp"),
        P("tp"),
        P("tp", None),
        P(),
        P("sp", "tp"),
        P("sp", "tp"),
        P("tp", "sp"),
    )

    def mapped(function):
        return jax.shard_map(
            function, mesh=mesh, in_specs=placed, out_specs=P(("sp", "tp"), None), check_vma=False
        )

    if mesh.shape["sp"] == PAIR * LINE and mesh.shape["tp"] == COLUMNS:
        return mapped(fused_body)
    return mapped(plain_body)
```

profile of v0, /device:TPU:0, one launch (start us, length us, event | category | flops | bytes accessed | tf_op | source)
XLA Modules:
  0.0 269.7 jit_solution(4161290317263609881)
XLA Ops:
  0.0 0.1 pad.3.clone
  0.1 0.1 dynamic_slice.14
  0.2 1.0 fusion
  1.1 0.1 pad.7.clone
  1.2 0.8 constant_dynamic-slice_fusion.1
  2.0 0.1 copy.22
  2.1 0.2 fusion.8
  2.3 0.2 multiply_cosine_fusion
  2.5 0.9 fusion.2
  3.5 0.7 maximum_maximum_fusion.1.lat_ref
  4.2 1.2 copy.19
  5.5 0.1 maximum_maximum_fusion
  5.6 1.0 copy.21.query_ref
  6.6 1.9 constant_dynamic-slice_fusion.resid_ref
  8.5 259.4 %shard_map.118 = bf16[64,4096]{1,0:T(8,128)(2,1)} custom-call(bf16[64,640]{1,0:T(8,128)(2,1)} %maximum_maximum_fusion.1.lat_ref, bf16[256,1024]{1,0:T(8,128)(2,1)} %copy.21.query_ref, bf16[64,4096]{1,0:T(8,128)(2,1)} %constant_dynamic-slice_fusion.resid_ref, f32[1,512]{1,0:T(1,128)} %bitcast.8, f32[1,4096]{1,0:T(1,128)} %bitcast.7, ...), custom_call_target="tpu_custom_call" | custom-call | tf_op jit(solution)/shard_map/pallas_call | solution.py:817
  267.9 1.9 copy.24
  (8 shorter events, 0.1 us)
where the time goes:
time: 270 us
  Pallas kernels  259 us (96%)
  local copies, waits for them, and re-layouts  7.03 us (3%)
  other arithmetic  3.23 us (1%)
    pallas_call x1, Pallas kernels, fused_body(): pl.pallas_call(whole_step, out_shape=jax.ShapeDtypeStruct((share, width),...  259 us

commit v1 on v0

--- a/solution.py
+++ b/solution.py
@@ -292,19 +292,28 @@
 MESH = pl.DeviceIdType.MESH
 
 
+ROW_ORDER = (1, 2, 0, 3)
+
+
 def whole_step(
-    lat_ref,
     query_ref,
-    resid_ref,
+    latent_ref,
+    rope_ref,
+    table_ref,
+    lat_gain_ref,
     out_gain_ref,
     ffn_gain_ref,
+    resid_hbm,
     kv_hbm,
     out_hbm,
     gate_hbm,
     up_hbm,
     down_hbm,
     result_ref,
+    lat_mine,
     lat_buf,
+    query,
+    resid,
     kv_w,
     out_w,
     gate_up,
@@ -320,8 +329,12 @@
     core_in,
     near_out,
     near_in,
-    line_out,
-    line_in,
+    partial_rows,
+    core_rows,
+    near_rows_out,
+    near_rows_in,
+    rows_out,
+    rows_in,
     middle,
     total,
     local_sem,
@@ -333,6 +346,8 @@
     turn_recv,
     pair_send,
     pair_recv,
+    down_send,
+    down_recv,
     act_line_send,
     act_line_recv,
     act_spread_send,
@@ -343,19 +358,26 @@
     core_recv,
     near_send,
     near_recv,
-    line_send,
-    line_recv,
+    hid_send,
+    hid_pass_send,
+    hid_recv,
+    core_rows_send,
+    core_rows_recv,
+    near_rows_send,
+    near_rows_recv,
+    rows_send,
+    rows_recv,
 ):
     rank = lax.axis_index("sp")
     col = lax.axis_index("tp")
     ranks = lat_buf.shape[0]
     rows = lat_buf.shape[1]
-    share = lat_ref.shape[0]
-    width = resid_ref.shape[1]
-    units = hidden.shape[1]
+    share = lat_mine.shape[0]
+    width = resid.shape[1]
+    units = hidden.shape[1] // LINE
     block = gate_hbm.shape[0]
     latent = kv_w.shape[0]
-    heads = query_ref.shape[1] // (2 * LANES)
+    heads = query.shape[0]
     z = rank // PAIR
     x = rank % PAIR
     mate = z * PAIR + (PAIR - 1 - x)
@@ -381,6 +403,30 @@
             pl.when(when)(copy.start)
         pending.append((copy, when))
 
+    def local(src, dst, slot):
+        copy = pltpu.make_async_copy(src, dst, local_sem.at[slot])
+        copy.start()
+        return copy
+
+    own_rows = pl.ds(pl.multiple_of(col * share, share), share)
+    kv_copy = local(kv_hbm, kv_w, 0)
+    out_copy = local(out_hbm, out_w, 1)
+    resid_copy = local(resid_hbm.at[own_rows, :], resid, 2)
+
+    def turned(values, cosine, sine):
+        half = values.shape[1] // 2
+        swapped = jnp.concatenate([values[:, half:], values[:, :half]], axis=1)
+        return values * cosine + swapped * sine
+
+    wide = latent_ref[own_rows, :].astype(jnp.float32)
+    wide = wide * lax.rsqrt(jnp.mean(wide * wide, axis=1, keepdims=True) + EPSILON)
+    lat_mine[:, :latent] = (wide * lat_gain_ref[...]).astype(jnp.bfloat16)
+    key_rope = turned(
+        rope_ref[own_rows, :].astype(jnp.float32), table_ref[own_rows, :ROPE],
+        table_ref[own_rows, ROPE:],
+    ).astype(jnp.bfloat16)
+    lat_mine[:, latent:] = jnp.concatenate([key_rope, jnp.zeros_like(key_rope)], axis=1)
+
     barrier = pltpu.get_barrier_semaphore()
     for step in range(1, ranks):
         pl.semaphore_signal(
@@ -403,35 +449,26 @@
     for step in range(1, ranks):
         send(
             remote(
-                lat_ref, lat_piece(rank, col), lat_send.at[step - 1], lat_recv.at[rank],
+                lat_mine, lat_piece(rank, col), lat_send.at[step - 1], lat_recv.at[rank],
                 sp=(rank + step) % ranks,
             ),
             rank + step < ranks,
         )
-    lat_spread(rank, lat_ref, 2, 2).start()
-    lat_spread(rank, lat_ref, 1, 1).start()
-    lat_buf[rank, pl.ds(pl.multiple_of(col * share, share), share), :] = lat_ref[...]
+    lat_spread(rank, lat_mine, 2, 2).start()
+    lat_spread(rank, lat_mine, 1, 1).start()
+    lat_buf[rank, own_rows, :] = lat_mine[...]
 
     def region(kind, source):
         at = pl.multiple_of(source * block, block)
-        if kind == 2:
-            return down.at[:, pl.ds(at, block)]
         return gate_up.at[pl.ds(at, block), pl.ds(kind * units, units)]
 
     def own_part(kind, place):
         at = pl.multiple_of(place * units, units)
-        if kind == 2:
-            return down_hbm.at[pl.ds(at, units), :]
         return (gate_hbm, up_hbm)[kind].at[:, pl.ds(at, units)]
 
-    def local(src, dst, slot):
-        copy = pltpu.make_async_copy(src, dst, local_sem.at[slot])
-        copy.start()
-        return copy
-
-    kv_copy = local(kv_hbm, kv_w, 0)
-    out_copy = local(out_hbm, out_w, 1)
-    own_copies = [local(own_part(kind, z), region(kind, rank), 2 + kind) for kind in range(3)]
+    def down_part(half):
+        middle_row = down_hbm.shape[0] // 2
+        return pl.ds(half * middle_row, middle_row)
 
     def turn(kind):
         for k in range(1, LINE):
@@ -457,15 +494,39 @@
         for k in range(LINE):
             arrived(region(kind, z_flips[k] * PAIR + (PAIR - 1 - x)), pair_recv.at[kind, k])
 
+    down_own = pl.ds(pl.multiple_of(x * down_hbm.shape[1], LANES), down_hbm.shape[1])
+    down_mate = pl.ds(
+        pl.multiple_of((PAIR - 1 - x) * down_hbm.shape[1], LANES), down_hbm.shape[1]
+    )
+
+    def pump_down(half):
+        send(
+            remote(
+                down_hbm.at[down_part(half), :], down.at[down_part(half), down_own],
+                down_send.at[half], down_recv.at[half], sp=mate,
+            )
+        )
+
     turn(0)
     turn(1)
     pump(0, 0)
     pump(1, 0)
-
+    pump_down(0)
+    own_copies = [local(own_part(kind, z), region(kind, rank), 3 + kind) for kind in range(2)]
+    own_copies.append(local(down_hbm, down.at[:, down_own], 5))
+
+    for head in range(heads):
+        at = head * (NOPE + ROPE)
+        rotary = turned(
+            query_ref[:, at + NOPE : at + NOPE + ROPE].astype(jnp.float32), table_ref[:, :ROPE],
+            table_ref[:, ROPE:],
+        ).astype(jnp.bfloat16)
+        query[head, :, :NOPE] = query_ref[:, at : at + NOPE]
+        query[head, :, NOPE:] = jnp.concatenate([rotary, jnp.zeros_like(rotary)], axis=1)
     top[...] = jnp.full(top.shape, LOWEST, jnp.float32)
     norm[...] = jnp.zeros(norm.shape, jnp.float32)
     acc[...] = jnp.zeros(acc.shape, jnp.float32)
-    scale = 1.0 / math.sqrt(NOPE + ROPE)
+    scale = math.log2(math.e) / math.sqrt(NOPE + ROPE)
     kv_copy.wait()
 
     def attend(index, carry):
@@ -492,14 +553,13 @@
             at = head * (NOPE + VDIM)
             keys = jnp.concatenate([key_value[:, at : at + NOPE], key_rope], axis=1)
             scores = lax.dot_general(
-                query_ref[:, head * 2 * LANES : (head + 1) * 2 * LANES], keys,
-                (((1,), (1,)), ((), ())), preferred_element_type=jnp.float32,
+                query[head], keys, (((1,), (1,)), ((), ())), preferred_element_type=jnp.float32
             )
             scores = jnp.where(allowed, scores * scale, LOWEST)
             old = top[head]
             new = jnp.maximum(old, jnp.max(scores, axis=1, keepdims=True))
-            weights = jnp.exp(scores - new[:, :1])
-            fade = jnp.exp(old - new)
+            weights = jnp.exp2(scores - new[:, :1])
+            fade = jnp.exp2(old - new)
             top[head] = new
             norm[head] = norm[head] * fade + jnp.sum(weights, axis=1, keepdims=True)
             across = slice(head * VDIM, (head + 1) * VDIM)
@@ -510,8 +570,6 @@
         return carry
 
     lax.fori_loop(0, rank + 1, attend, 0)
-    for kind, k in ((0, 1), (1, 1), (0, 2)):
-        pump(kind, k)
 
     squares = jnp.zeros((rows, 1), jnp.float32)
     attended = []
@@ -524,75 +582,62 @@
     stats_mine[...] = jnp.broadcast_to(squares, stats_mine.shape)
 
     chunk = 4 * LANES
-    chunks = width // chunk
-
-    def piece_of(ref, slot, column):
-        return ref.at[slot, pl.ds(pl.multiple_of(column * share, share), share), :]
-
-    def project(slot, left, right):
+
+    def piece_of(ref, column):
+        return ref.at[pl.ds(pl.multiple_of(column * share, share), share), :]
+
+    def project(left, right, target):
         def one(index, carry):
             at = pl.ds(pl.multiple_of(index * chunk, chunk), chunk)
-            partial[slot, :, at] = jnp.dot(
+            target[:, at] = jnp.dot(
                 left, right[:, at], preferred_element_type=jnp.float32
             ).astype(jnp.bfloat16)
             return carry
 
-        lax.fori_loop(0, chunks, one, 0)
-
-    def each_chunk(work):
+        lax.fori_loop(0, right.shape[1] // chunk, one, 0)
+
+    def each_chunk(across, work):
         def one(index, carry):
             work(pl.ds(pl.multiple_of(index * chunk, chunk), chunk))
             return carry
 
-        lax.fori_loop(0, chunks, one, 0)
-
-    def fold(slot):
-        send(
-            remote(
-                piece_of(partial, slot, col_flips[3]), core_in.at[slot, 1],
-                core_send.at[slot, 1], core_recv.at[slot, 1], tp=col_flips[1],
+        lax.fori_loop(0, across // chunk, one, 0)
+
+    def fold(part, core, out, near, sems):
+        core_s, core_r, near_s, near_r = sems
+        for slot, column in ((1, 3), (0, 1)):
+            send(
+                remote(
+                    piece_of(part, col_flips[column]), core.at[slot], core_s.at[slot],
+                    core_r.at[slot], tp=col_flips[1],
+                )
             )
-        )
-        send(
-            remote(
-                piece_of(partial, slot, col_flips[1]), core_in.at[slot, 0],
-                core_send.at[slot, 0], core_recv.at[slot, 0], tp=col_flips[1],
+        arrived(core.at[1], core_r.at[1])
+        theirs = pl.ds(pl.multiple_of(col_flips[2] * share, share), share)
+
+        def add(at):
+            out[:, at] = (
+                part[theirs, at].astype(jnp.float32) + core[1, :, at].astype(jnp.float32)
+            ).astype(jnp.bfloat16)
+
+        each_chunk(out.shape[1], add)
+        send(remote(out, near, near_s, near_r, tp=col_flips[2]))
+        arrived(core.at[0], core_r.at[0])
+
+    def folded(part, core, near, sems, keep):
+        arrived(near, sems[3])
+
+        def add(at):
+            keep(
+                at,
+                part[own_rows, at].astype(jnp.float32)
+                + core[0, :, at].astype(jnp.float32)
+                + near[:, at].astype(jnp.float32),
             )
-        )
-        arrived(core_in.at[slot, 1], core_recv.at[slot, 1])
-
-        def add(at):
-            theirs = partial[
-                slot, pl.ds(pl.multiple_of(col_flips[2] * share, share), share), at
-            ].astype(jnp.float32)
-            near_out[slot, :, at] = (theirs + core_in[slot, 1, :, at].astype(jnp.float32)).astype(
-                jnp.bfloat16
-            )
-
-        each_chunk(add)
-        send(
-            remote(
-                near_out.at[slot], near_in.at[slot], near_send.at[slot], near_recv.at[slot],
-                tp=col_flips[2],
-            )
-        )
-        arrived(core_in.at[slot, 0], core_recv.at[slot, 0])
-
-    def folded(slot):
-        arrived(near_in.at[slot], near_recv.at[slot])
-
-        def add(at):
-            mine = partial[slot, pl.ds(pl.multiple_of(col * share, share), share), at]
-            total[:, at] = (
-                mine.astype(jnp.float32)
-                + core_in[slot, 0, :, at].astype(jnp.float32)
-                + near_in[slot, :, at].astype(jnp.float32)
-            )
-
-        each_chunk(add)
+
+        each_chunk(near.shape[1], add)
 
     out_copy.wait()
-    first = LINE
     for m in range(1, COLUMNS):
         send(
             remote(
@@ -600,20 +645,26 @@
                 stats_in.at[m - 1], stat_send.at[m - 1], stat_recv.at[m - 1], tp=col_flips[m],
             )
         )
-    project(first, attended, out_w)
-    fold(first)
-    for kind, k in ((1, 2), (0, 3)):
-        pump(kind, k)
-    squares = stats_mine[pl.ds(pl.multiple_of(col * share, share), share), :]
+    project(attended, out_w, partial)
+    first = (core_send, core_recv, near_send.at[0], near_recv.at[0])
+    fold(partial, core_in, near_out, near_in, first)
+    for k in range(1, LINE):
+        pump(0, k)
+    squares = stats_mine[own_rows, :]
     for m in range(1, COLUMNS):
         arrived(stats_in.at[m - 1], stat_recv.at[m - 1])
         squares = squares + stats_in[m - 1]
     factor = lax.rsqrt(squares / (HEADS * VDIM) + EPSILON)[:, :1]
-    folded(first)
+
+    def keep_total(at, values):
+        total[:, at] = values
+
+    folded(partial, core_in, near_in, first, keep_total)
+    resid_copy.wait()
     squares = jnp.zeros((share, 1), jnp.float32)
-    for index in range(chunks):
+    for index in range(width // chunk):
         at = slice(index * chunk, (index + 1) * chunk)
-        mid = (resid_ref[:, at].astype(jnp.float32) + total[:, at] * factor).astype(jnp.bfloat16)
+        mid = (resid[:, at].astype(jnp.float32) + total[:, at] * factor).astype(jnp.bfloat16)
         middle[:, at] = mid
         mid = mid.astype(jnp.float32)
         squares = squares + jnp.sum(mid * mid, axis=1, keepdims=True)
@@ -623,10 +674,10 @@
         at = pl.multiple_of(place * rows + column * share, share)
         return act.at[pl.ds(at, share), :]
 
-    own_rows = pl.ds(pl.multiple_of(z * rows + col * share, share), share)
-    for index in range(chunks):
+    at_own = pl.ds(pl.multiple_of(z * rows + col * share, share), share)
+    for index in range(width // chunk):
         at = slice(index * chunk, (index + 1) * chunk)
-        act[own_rows, at] = (
+        act[at_own, at] = (
             middle[:, at].astype(jnp.float32) * factor * ffn_gain_ref[:, at]
         ).astype(jnp.bfloat16)
 
@@ -636,123 +687,183 @@
     def down_line(src, dst, send_sem, recv_sem, when):
         send(remote(src, dst, send_sem, recv_sem, sp=(rank + ranks - PAIR) % ranks), when)
 
-    def act_spread(place, index, flip, slot):
+    def act_spread(place, flip, slot):
         piece = act_piece(place, col_flips[slot - flip])
         send(
             remote(
-                piece, piece, act_spread_send.at[index, slot - 1],
-                act_spread_recv.at[index, slot - 1], tp=col_flips[flip],
+                piece, piece, act_spread_send.at[place, slot - 1],
+                act_spread_recv.at[place, slot - 1], tp=col_flips[flip],
             )
         )
 
     mine = act_piece(z, col)
     up_line(mine, mine, act_line_send.at[0], act_line_recv.at[z], z < LINE - 1)
     down_line(mine, mine, act_line_send.at[1], act_line_recv.at[z], z > 0)
-    act_spread(z, 0, 2, 2)
-    act_spread(z, 0, 1, 1)
-    pump(1, 3)
+    act_spread(z, 2, 2)
+    act_spread(z, 1, 1)
     order = [
         z,
         z_flips[1],
         z_flips[2] * (1 - inner) + z_flips[3] * inner,
         z_flips[3] * (1 - inner) + z_flips[2] * inner,
     ]
-    for index in range(LINE):
-        place = order[index]
-        if index < LINE - 1:
-            nearer = order[index + 1]
-            piece = act_piece(nearer, col)
-            arrived(piece, act_line_recv.at[nearer])
-            up_line(
-                piece, piece, act_line_send.at[2 + 2 * index], act_line_recv.at[nearer],
-                (nearer < z) & (z < LINE - 1),
-            )
-            down_line(
-                piece, piece, act_line_send.at[3 + 2 * index], act_line_recv.at[nearer],
-                (nearer > z) & (z > 0),
-            )
-            act_spread(nearer, index + 1, 2, 2)
-            act_spread(nearer, index + 1, 1, 1)
-        if index == LINE - 2:
-            turn(2)
-            pump(2, 0)
-        if index == 0:
-            own_copies[0].wait()
-            own_copies[1].wait()
-            paired(0)
-            paired(1)
-        arrived(act_piece(place, col_flips[2]), act_spread_recv.at[index, 1])
-        act_spread(place, index, 1, 3)
-        arrived(act_piece(place, col_flips[1]), act_spread_recv.at[index, 0])
-        arrived(act_piece(place, col_flips[3]), act_spread_recv.at[index, 2])
-        here = pl.ds(pl.multiple_of(place * rows, rows), rows)
+
+    def near_act(place):
+        arrived(act_piece(place, col_flips[2]), act_spread_recv.at[place, 1])
+        act_spread(place, 1, 3)
+
+    for index in range(1, LINE):
+        nearer = order[index]
+        piece = act_piece(nearer, col)
+        arrived(piece, act_line_recv.at[nearer])
+        up_line(
+            piece, piece, act_line_send.at[2 * index], act_line_recv.at[nearer],
+            (nearer < z) & (z < LINE - 1),
+        )
+        down_line(
+            piece, piece, act_line_send.at[2 * index + 1], act_line_recv.at[nearer],
+            (nearer > z) & (z > 0),
+        )
+        act_spread(nearer, 2, 2)
+        act_spread(nearer, 1, 1)
+        near_act(order[index - 1])
+        if index == 1:
+            pump(1, 1)
+        elif index == 2:
+            pump(1, 2)
+            pump(1, 3)
+            pump_down(1)
+
+    for copy in own_copies:
+        copy.wait()
+    paired(0)
+    paired(1)
+
+    def hid_piece(place, source):
+        return hidden.at[
+            pl.ds(place * rows, rows), pl.ds(pl.multiple_of(source * units, units), units)
+        ]
+
+    def gated(index):
+        place = ROW_ORDER[index]
+        arrived(act_piece(place, col_flips[1]), act_spread_recv.at[place, 0])
+        arrived(act_piece(place, col_flips[3]), act_spread_recv.at[place, 2])
+        here = slice(place * rows, (place + 1) * rows)
         both = jnp.dot(act[here, :], gate_up[...], preferred_element_type=jnp.float32)
         gate = both[:, :units]
-        hidden[here, :] = (gate / (1.0 + jnp.exp(-gate)) * both[:, units:]).astype(jnp.bfloat16)
-
-    for k in range(1, LINE):
-        pump(2, k)
-    own_copies[2].wait()
-    paired(2)
-
-    def start_rows(slot):
-        place = z_flips[LINE - 1 - slot]
-        left = hidden[pl.ds(pl.multiple_of(place * rows, rows), rows), :]
-        project(slot, left, down)
-        fold(slot)
-
-    def add_line(slot):
-        def add(at):
-            total[:, at] = total[:, at] + line_in[slot, :, at].astype(jnp.float32)
-
-        each_chunk(add)
-
-    def pass_rows(slot):
-        place = z_flips[LINE - 1 - slot]
-        folded(slot)
-
-        @pl.when(((place > z) & (z > 0)) | ((place < z) & (z < LINE - 1)))
+        hidden[here, pl.ds(pl.multiple_of(z * units, units), units)] = (
+            gate / (1.0 + jnp.exp(-gate)) * both[:, units:]
+        ).astype(jnp.bfloat16)
+        piece = hid_piece(place, z)
+        up_line(piece, piece, hid_send.at[index, 0], hid_recv.at[place, z], z < LINE - 1)
+        down_line(piece, piece, hid_send.at[index, 1], hid_recv.at[place, z], z > 0)
+
+    def pass_hidden(index, distance):
+        place = ROW_ORDER[index]
+        for side, source, when in (
+            (0, z - distance, (z - distance >= 0) & (z < LINE - 1)),
+            (1, z + distance, (z + distance < LINE) & (z > 0)),
+        ):
+            source = (source + LINE) % LINE
+            piece = hid_piece(place, source)
+            copy = remote(
+                piece, piece, hid_pass_send.at[index, distance - 1, side],
+                hid_recv.at[place, source],
+                sp=((rank + PAIR) if side == 0 else (rank + ranks - PAIR)) % ranks,
+            )
+
+            @pl.when(when)
+            def _():
+                arrived(piece, hid_recv.at[place, source])
+                copy.start()
+
+            pending.append((copy, when))
+
+    def hidden_all(index):
+        place = ROW_ORDER[index]
+        for distance in range(1, LINE):
+            for source, when in (
+                (LINE - 1 - distance, z == LINE - 1),
+                (distance, z == 0),
+            ):
+
+                @pl.when(when)
+                def _():
+                    arrived(hid_piece(place, source), hid_recv.at[place, source])
+
+    def row_sems(index):
+        return (
+            core_rows_send.at[index], core_rows_recv.at[index], near_rows_send.at[index],
+            near_rows_recv.at[index],
+        )
+
+    def start_rows(index):
+        place = ROW_ORDER[index]
+        hidden_all(index)
+        project(hidden[place * rows : (place + 1) * rows, :], down, partial_rows.at[index])
+        fold(
+            partial_rows.at[index], core_rows.at[index], near_rows_out.at[index],
+            near_rows_in.at[index], row_sems(index),
+        )
+
+    def end_rows(index):
+        place = ROW_ORDER[index]
+
+        def keep(at, values):
+            rows_out[index, :, at] = values.astype(jnp.bfloat16)
+
+        folded(
+            partial_rows.at[index], core_rows.at[index], near_rows_in.at[index], row_sems(index),
+            keep,
+        )
+        send(
+            remote(
+                rows_out.at[index], rows_in.at[z], rows_send.at[index], rows_recv.at[z],
+                sp=place * PAIR + x,
+            ),
+            z != place,
+        )
+
+        @pl.when(z == place)
         def _():
-            arrived(line_in.at[place], line_recv.at[place])
-            add_line(place)
-
-        def keep(at):
-            line_out[slot, :, at] = total[:, at].astype(jnp.bfloat16)
-
-        each_chunk(keep)
-        up_line(
-            line_out.at[slot], line_in.at[place], line_send.at[slot, 0], line_recv.at[place],
-            place > z,
-        )
-        last = jnp.where(place == z - 1, LINE, place)
-        down_line(
-            line_out.at[slot], line_in.at[last], line_send.at[slot, 1], line_recv.at[last],
-            place < z,
-        )
-
+            rows_in[z] = rows_out[index]
+
+
+    gated(0)
+    gated(1)
+    near_act(order[LINE - 1])
+    pass_hidden(0, 1)
+    gated(2)
+    pass_hidden(1, 1)
+    pass_hidden(0, 2)
+    gated(3)
+    pass_hidden(2, 1)
+    pass_hidden(1, 2)
+    for half in range(2):
+        arrived(down.at[down_part(half), down_mate], down_recv.at[half])
     start_rows(0)
+    pass_hidden(3, 1)
+    pass_hidden(2, 2)
     start_rows(1)
-    pass_rows(0)
+    end_rows(0)
+    pass_hidden(3, 2)
     start_rows(2)
-    pass_rows(1)
+    end_rows(1)
     start_rows(3)
-    pass_rows(2)
-    folded(LINE - 1)
-
-    @pl.when(z > 0)
-    def _():
-        arrived(line_in.at[z], line_recv.at[z])
-        add_line(z)
-
-    @pl.when(z < LINE - 1)
-    def _():
-        arrived(line_in.at[LINE], line_recv.at[LINE])
-        add_line(LINE)
-
-    def finish(at):
-        result_ref[:, at] = (middle[:, at].astype(jnp.float32) + total[:, at]).astype(jnp.bfloat16)
-
-    each_chunk(finish)
+    end_rows(2)
+    end_rows(3)
+    for source in range(LINE):
+
+        @pl.when(z != source)
+        def _():
+            arrived(rows_in.at[source], rows_recv.at[source])
+
+    part = rows_in.shape[2]
+    for source in range(LINE):
+        at = slice(source * part, (source + 1) * part)
+        result_ref[:, at] = (
+            middle[:, at].astype(jnp.float32) + rows_in[source].astype(jnp.float32)
+        ).astype(jnp.bfloat16)
 
     for copy, when in pending:
         if when is None:
@@ -787,90 +898,101 @@
     down_weight,
 ):
     ranks, columns = lax.axis_size("sp"), lax.axis_size("tp")
-    rank, column = lax.axis_index("sp"), lax.axis_index("tp")
+    rank = lax.axis_index("sp")
     rows, width = resid.shape
     share = rows // columns
     heads = queries.shape[1] // (NOPE + ROPE)
     units = gate_weight.shape[1] // LINE
     block = gate_weight.shape[0]
-    own_first = column * share
-    first_row = rank * rows
-
-    def mine(values):
-        return lax.dynamic_slice_in_dim(values, own_first, share, 0)
-
-    places = (first_row + jnp.arange(rows, dtype=jnp.int32)).astype(jnp.float32)
-    normed = norm_rows(mine(latent), lat_gain).astype(jnp.bfloat16)
-    key_rope = rotate(mine(rope_key).astype(jnp.float32), mine(places)).astype(jnp.bfloat16)
-    message = jnp.concatenate([normed, key_rope, jnp.zeros_like(key_rope)], axis=1)
-    query = queries.reshape(rows, heads, NOPE + ROPE)
-    query_rope = rotate(query[:, :, NOPE:].astype(jnp.float32), places[:, None]).astype(
-        jnp.bfloat16
-    )
-    query = jnp.concatenate([query[:, :, :NOPE], query_rope, jnp.zeros_like(query_rope)], axis=2)
-    query = query.reshape(rows, heads * 2 * LANES)
+    depth = latent.shape[1]
+    places = (rank * rows + jnp.arange(rows, dtype=jnp.int32)).astype(jnp.float32)
+    half = ROPE // 2
+    inverse = THETA ** (-jnp.arange(half, dtype=jnp.float32) / half)
+    angle = places[:, None] * inverse
+    cosine, sine = jnp.cos(angle), jnp.sin(angle)
+    table = jnp.concatenate([cosine, cosine, -sine, sine], axis=1)
     bf, f32 = jnp.bfloat16, jnp.float32
     dma = pltpu.SemaphoreType.DMA
-    slots = LINE + 1
     vmem = pl.BlockSpec(memory_space=pltpu.VMEM)
     anywhere = pl.BlockSpec(memory_space=pl.ANY)
+    part = width // LINE
+    others = columns - 1
     return pl.pallas_call(
         whole_step,
         out_shape=jax.ShapeDtypeStruct((share, width), bf),
-        in_specs=[vmem] * 5 + [anywhere] * 5,
+        in_specs=[vmem] * 7 + [anywhere] * 6,
         out_specs=vmem,
         scratch_shapes=[
-            pltpu.VMEM((ranks, rows, message.shape[1]), bf),
+            pltpu.VMEM((share, depth + LANES), bf),
+            pltpu.VMEM((ranks, rows, depth + LANES), bf),
+            pltpu.VMEM((heads, rows, 2 * LANES), bf),
+            pltpu.VMEM((share, width), bf),
             pltpu.VMEM(kv_weight.shape, bf),
             pltpu.VMEM(out_weight.shape, bf),
             pltpu.VMEM((ranks * block, 2 * units), bf),
-            pltpu.VMEM((units, ranks * down_weight.shape[1]), bf),
+            pltpu.VMEM((LINE * units, PAIR * down_weight.shape[1]), bf),
             pltpu.VMEM((LINE * rows, width), bf),
-            pltpu.VMEM((LINE * rows, units), bf),
+            pltpu.VMEM((LINE * rows, LINE * units), bf),
             pltpu.VMEM((heads, rows, LANES), f32),
             pltpu.VMEM((heads, rows, LANES), f32),
             pltpu.VMEM((rows, heads * VDIM), f32),
             pltpu.VMEM((rows, LANES), f32),
-            pltpu.VMEM((columns - 1, share, LANES), f32),
-            pltpu.VMEM((slots, rows, width), bf),
-            pltpu.VMEM((slots, 2, share, width), bf),
-            pltpu.VMEM((slots, share, width), bf),
-            pltpu.VMEM((slots, share, width), bf),
-            pltpu.VMEM((LINE, share, width), bf),
-            pltpu.VMEM((slots, share, width), bf),
+            pltpu.VMEM((others, share, LANES), f32),
+            pltpu.VMEM((rows, width), bf),
+            pltpu.VMEM((2, share, width), bf),
+            pltpu.VMEM((share, width), bf),
+            pltpu.VMEM((share, width), bf),
+            pltpu.VMEM((LINE, rows, part), bf),
+            pltpu.VMEM((LINE, 2, share, part), bf),
+            pltpu.VMEM((LINE, share, part), bf),
+            pltpu.VMEM((LINE, share, part), bf),
+            pltpu.VMEM((LINE, share, part), bf),
+            pltpu.VMEM((LINE, share, part), bf),
             pltpu.VMEM((share, width), bf),
             pltpu.VMEM((share, width), f32),
-            dma((5,)),
+            dma((6,)),
             dma((ranks - 1,)),
             dma((ranks,)),
-            dma((ranks, columns - 1)),
-            dma((ranks, columns - 1)),
-            dma((3, LINE)),
-            dma((3, LINE)),
-            dma((3, LINE)),
-            dma((3, LINE)),
+            dma((ranks, others)),
+            dma((ranks, others)),
+            dma((2, LINE)),
+            dma((2, LINE)),
+            dma((2, LINE)),
+            dma((2, LINE)),
+            dma((2,)),
+            dma((2,)),
             dma((2 * LINE,)),
             dma((LINE,)),
-            dma((LINE, columns - 1)),
-            dma((LINE, columns - 1)),
-            dma((columns - 1,)),
-            dma((columns - 1,)),
-            dma((slots, 2)),
-            dma((slots, 2)),
-            dma((slots,)),
-            dma((slots,)),
+            dma((LINE, others)),
+            dma((LINE, others)),
+            dma((others,)),
+            dma((others,)),
+            dma((2,)),
+            dma((2,)),
+            dma((1,)),
+            dma((1,)),
             dma((LINE, 2)),
-            dma((slots,)),
+            dma((LINE, 2, 2)),
+            dma((LINE, LINE)),
+            dma((LINE, 2)),
+            dma((LINE, 2)),
+            dma((LINE,)),
+            dma((LINE,)),
+            dma((LINE,)),
+            dma((LINE,)),
         ],
         compiler_params=pltpu.CompilerParams(
             collective_id=0, has_side_effects=True, vmem_limit_bytes=66 * 1024 * 1000
         ),
     )(
-        message,
-        query,
-        mine(resid),
+        queries,
+        latent,
+        rope_key,
+        table,
+        lat_gain.reshape(1, -1),
         out_gain.reshape(1, -1),
         ffn_gain.reshape(1, -1),
+        resid,
         kv_weight,
         out_weight,
         gate_weight,

time: 270 us -> 198 us (0.73)
  Pallas kernels: 259 us -> 193 us
  local copies, waits for them, and re-layouts: 7.03 us -> 3.37 us
    pallas_call x1, Pallas kernels: 259 us -> 193 us  [fused_body(): pl.pallas_call(whole_step, out_shape=jax.ShapeDtypeStruct((share, width),...]
    dynamic_slice x3 -> x0, local copies, waits for them, and re-layouts: 2.73 us -> none  [mine(): return lax.dynamic_slice_in_dim(values, own_first, share, 0)]
where the time goes in v1:
time: 198 us
  Pallas kernels  193 us (97%)
  local copies, waits for them, and re-layouts  3.37 us (2%)
    pallas_call x1, Pallas kernels, fused_body(): pl.pallas_call(whole_step, out_shape=jax.ShapeDtypeStruct((share, width),...  193 us

profile of v1, /device:TPU:0, one launch (start us, length us, event | category | flops | bytes accessed | tf_op | source)
XLA Modules:
  0.0 197.9 jit_solution(11449736351763646866)
XLA Ops:
  0.0 1.5 copy.15.rope_ref
  1.5 0.5 multiply_cosine_fusion
  2.1 0.8 pad_maximum_fusion.table_ref
  2.9 193.2 %shard_map.118 = bf16[64,4096]{1,0:T(8,128)(2,1)} custom-call(bf16[256,768]{1,0:T(8,128)(2,1)} %query_ref.1, bf16[256,512]{1,0:T(8,128)(2,1)} %latent_ref.1, bf16[256,64]{1,0:T(8,128)(2,1)} %copy.15.rope_ref, f32[256,128]{1,0:T(8,128)} %pad_maximum_fusion.table_ref, f32[1,512]{1,0:T(1,128)} %bitcast.4, f32[1,512]{1,0:T(1,128)} %bitcast.5, ...), custom_call_target="tpu_custom_call" | custom-call | tf_op jit(solution)/shard_map/pallas_call | solution.py:920
  196.1 1.9 copy.17
  (2 shorter events, 0.0 us)

commit v2 on v1

--- a/solution.py
+++ b/solution.py
@@ -1,3 +1,4 @@
+import functools
 import math
 
 import jax
@@ -292,7 +293,7 @@
 MESH = pl.DeviceIdType.MESH
 
 
-ROW_ORDER = (1, 2, 0, 3)
+PARTS = 4
 
 
 def whole_step(
@@ -648,8 +649,7 @@
     project(attended, out_w, partial)
     first = (core_send, core_recv, near_send.at[0], near_recv.at[0])
     fold(partial, core_in, near_out, near_in, first)
-    for k in range(1, LINE):
-        pump(0, k)
+    pump(0, 1)
     squares = stats_mine[own_rows, :]
     for m in range(1, COLUMNS):
         arrived(stats_in.at[m - 1], stat_recv.at[m - 1])
@@ -670,9 +670,11 @@
         squares = squares + jnp.sum(mid * mid, axis=1, keepdims=True)
     factor = lax.rsqrt(squares / width + EPSILON)
 
-    def act_piece(place, column):
+    slab = width // PARTS
+
+    def act_piece(place, column, part):
         at = pl.multiple_of(place * rows + column * share, share)
-        return act.at[pl.ds(at, share), :]
+        return act.at[pl.ds(at, share), pl.ds(part * slab, slab)]
 
     at_own = pl.ds(pl.multiple_of(z * rows + col * share, share), share)
     for index in range(width // chunk):
@@ -687,84 +689,90 @@
     def down_line(src, dst, send_sem, recv_sem, when):
         send(remote(src, dst, send_sem, recv_sem, sp=(rank + ranks - PAIR) % ranks), when)
 
-    def act_spread(place, flip, slot):
-        piece = act_piece(place, col_flips[slot - flip])
+    def act_spread(place, flip, slot, part):
+        piece = act_piece(place, col_flips[slot - flip], part)
         send(
             remote(
-                piece, piece, act_spread_send.at[place, slot - 1],
-                act_spread_recv.at[place, slot - 1], tp=col_flips[flip],
-            )
-        )
-
-    mine = act_piece(z, col)
-    up_line(mine, mine, act_line_send.at[0], act_line_recv.at[z], z < LINE - 1)
-    down_line(mine, mine, act_line_send.at[1], act_line_recv.at[z], z > 0)
-    act_spread(z, 2, 2)
-    act_spread(z, 1, 1)
-    order = [
-        z,
-        z_flips[1],
-        z_flips[2] * (1 - inner) + z_flips[3] * inner,
-        z_flips[3] * (1 - inner) + z_flips[2] * inner,
-    ]
-
-    def near_act(place):
-        arrived(act_piece(place, col_flips[2]), act_spread_recv.at[place, 1])
-        act_spread(place, 1, 3)
-
-    for index in range(1, LINE):
+                piece, piece, act_spread_send.at[place, slot - 1, part],
+                act_spread_recv.at[place, slot - 1, part], tp=col_flips[flip],
+            )
+        )
+
+    def act_line(place, index, part, up, lower):
+        piece = act_piece(place, col, part)
+        recv = act_line_recv.at[place, part]
+        up_line(piece, piece, act_line_send.at[2 * index, part], recv, up)
+        down_line(piece, piece, act_line_send.at[2 * index + 1, part], recv, lower)
+        act_spread(place, 2, 2, part)
+        act_spread(place, 1, 1, part)
+
+    for part in range(PARTS):
+        act_line(z, 0, part, z < LINE - 1, z > 0)
+    pump(0, 2)
+    pump(0, 3)
+
+    def arrival(at):
+        inside = ((at + 1) // 2) % 2
+        half, mirror = (at + 2) % LINE, LINE - 1 - at
+        return [
+            at,
+            at + 1 - 2 * (at % 2),
+            half * (1 - inside) + mirror * inside,
+            mirror * (1 - inside) + half * inside,
+        ]
+
+    order = arrival(z)
+
+    def near_act(place, part):
+        arrived(act_piece(place, col_flips[2], part), act_spread_recv.at[place, 1, part])
+        act_spread(place, 1, 3, part)
+
+    def next_act(index):
         nearer = order[index]
-        piece = act_piece(nearer, col)
-        arrived(piece, act_line_recv.at[nearer])
-        up_line(
-            piece, piece, act_line_send.at[2 * index], act_line_recv.at[nearer],
-            (nearer < z) & (z < LINE - 1),
-        )
-        down_line(
-            piece, piece, act_line_send.at[2 * index + 1], act_line_recv.at[nearer],
-            (nearer > z) & (z > 0),
-        )
-        act_spread(nearer, 2, 2)
-        act_spread(nearer, 1, 1)
-        near_act(order[index - 1])
-        if index == 1:
-            pump(1, 1)
-        elif index == 2:
-            pump(1, 2)
-            pump(1, 3)
-            pump_down(1)
-
-    for copy in own_copies:
-        copy.wait()
-    paired(0)
-    paired(1)
+        for part in range(PARTS):
+            arrived(act_piece(nearer, col, part), act_line_recv.at[nearer, part])
+            act_line(
+                nearer, index, part, (nearer < z) & (z < LINE - 1), (nearer > z) & (z > 0)
+            )
+            near_act(order[index - 1], part)
+
+    next_act(1)
+    for k in range(1, LINE):
+        pump(1, k)
+    pump_down(1)
+    next_act(2)
 
     def hid_piece(place, source):
         return hidden.at[
-            pl.ds(place * rows, rows), pl.ds(pl.multiple_of(source * units, units), units)
+            pl.ds(pl.multiple_of(place * rows, rows), rows),
+            pl.ds(pl.multiple_of(source * units, units), units),
         ]
 
     def gated(index):
-        place = ROW_ORDER[index]
-        arrived(act_piece(place, col_flips[1]), act_spread_recv.at[place, 0])
-        arrived(act_piece(place, col_flips[3]), act_spread_recv.at[place, 2])
-        here = slice(place * rows, (place + 1) * rows)
+        place = order[index]
+        for part in range(PARTS):
+            arrived(act_piece(place, col_flips[1], part), act_spread_recv.at[place, 0, part])
+            arrived(act_piece(place, col_flips[3], part), act_spread_recv.at[place, 2, part])
+        here = pl.ds(pl.multiple_of(place * rows, rows), rows)
         both = jnp.dot(act[here, :], gate_up[...], preferred_element_type=jnp.float32)
         gate = both[:, :units]
         hidden[here, pl.ds(pl.multiple_of(z * units, units), units)] = (
             gate / (1.0 + jnp.exp(-gate)) * both[:, units:]
         ).astype(jnp.bfloat16)
+
+    def leave(index):
+        place = order[index]
         piece = hid_piece(place, z)
         up_line(piece, piece, hid_send.at[index, 0], hid_recv.at[place, z], z < LINE - 1)
         down_line(piece, piece, hid_send.at[index, 1], hid_recv.at[place, z], z > 0)
 
     def pass_hidden(index, distance):
-        place = ROW_ORDER[index]
         for side, source, when in (
             (0, z - distance, (z - distance >= 0) & (z < LINE - 1)),
             (1, z + distance, (z + distance < LINE) & (z > 0)),
         ):
             source = (source + LINE) % LINE
+            place = arrival(source)[index]
             piece = hid_piece(place, source)
             copy = remote(
                 piece, piece, hid_pass_send.at[index, distance - 1, side],
@@ -779,8 +787,13 @@
 
             pending.append((copy, when))
 
+    upper = z // (LINE // 2)
+
+    def row_place(index):
+        return index * upper + (LINE - 1 - index) * (1 - upper)
+
     def hidden_all(index):
-        place = ROW_ORDER[index]
+        place = row_place(index)
         for distance in range(1, LINE):
             for source, when in (
                 (LINE - 1 - distance, z == LINE - 1),
@@ -798,16 +811,17 @@
         )
 
     def start_rows(index):
-        place = ROW_ORDER[index]
+        place = row_place(index)
         hidden_all(index)
-        project(hidden[place * rows : (place + 1) * rows, :], down, partial_rows.at[index])
+        here = pl.ds(pl.multiple_of(place * rows, rows), rows)
+        project(hidden[here, :], down, partial_rows.at[index])
         fold(
             partial_rows.at[index], core_rows.at[index], near_rows_out.at[index],
             near_rows_in.at[index], row_sems(index),
         )
 
     def end_rows(index):
-        place = ROW_ORDER[index]
+        place = row_place(index)
 
         def keep(at, values):
             rows_out[index, :, at] = values.astype(jnp.bfloat16)
@@ -829,24 +843,63 @@
             rows_in[z] = rows_out[index]
 
 
-    gated(0)
-    gated(1)
-    near_act(order[LINE - 1])
+    def weights_ready():
+        for copy in own_copies:
+            copy.wait()
+        paired(0)
+        paired(1)
+
+    outer = (z == 0) | (z == LINE - 1)
+
+    def early(first):
+        weights_ready()
+        for index in range(2):
+            gated(index)
+            place = order[index]
+            piece = hid_piece(place, z)
+            recv = hid_recv.at[place, z]
+            up = remote(
+                piece, piece, hid_send.at[index, 0], recv, sp=(rank + PAIR) % ranks
+            )
+            lower = remote(
+                piece, piece, hid_send.at[index, 1], recv, sp=(rank + ranks - PAIR) % ranks
+            )
+            if first:
+                pl.when(z == 0)(up.start)
+                pl.when(z > 0)(lower.start)
+            else:
+                up.start()
+                lower.start()
+
+    pl.when(outer)(functools.partial(early, True))
+    next_act(3)
+    pl.when(inner > 0)(functools.partial(early, False))
+    for index in range(2):
+        piece = hid_piece(order[index], z)
+        for side, when in ((0, z < LINE - 1), (1, z > 0)):
+            pending.append(
+                (remote(piece, piece, hid_send.at[index, side], hid_send.at[index, side],
+                        sp=mate), when)
+            )
+    gated(2)
+    leave(2)
+    for part in range(PARTS):
+        near_act(order[LINE - 1], part)
+    gated(3)
+    leave(3)
     pass_hidden(0, 1)
-    gated(2)
     pass_hidden(1, 1)
     pass_hidden(0, 2)
-    gated(3)
     pass_hidden(2, 1)
     pass_hidden(1, 2)
+    pass_hidden(3, 1)
+    pass_hidden(2, 2)
+    pass_hidden(3, 2)
     for half in range(2):
         arrived(down.at[down_part(half), down_mate], down_recv.at[half])
     start_rows(0)
-    pass_hidden(3, 1)
-    pass_hidden(2, 2)
     start_rows(1)
     end_rows(0)
-    pass_hidden(3, 2)
     start_rows(2)
     end_rows(1)
     start_rows(3)
@@ -961,10 +1014,10 @@
             dma((2, LINE)),
             dma((2,)),
             dma((2,)),
-            dma((2 * LINE,)),
-            dma((LINE,)),
-            dma((LINE, others)),
-            dma((LINE, others)),
+            dma((2 * LINE, PARTS)),
+            dma((LINE, PARTS)),
+            dma((LINE, others, PARTS)),
+            dma((LINE, others, PARTS)),
             dma((others,)),
             dma((others,)),
             dma((2,)),

time: 198 us -> 189 us (0.955); the launches traced: 198 us -> 185 us
  Pallas kernels: 193 us -> 181 us
    pallas_call x1, Pallas kernels: 193 us -> 181 us  [fused_body(): pl.pallas_call(whole_step, out_shape=jax.ShapeDtypeStruct((share, width),...]
where the time goes in v2:
time: 189 us; the launch traced here: 185 us
  Pallas kernels  181 us (96%)
  local copies, waits for them, and re-layouts  3.37 us (2%)
    pallas_call x1, Pallas kernels, fused_body(): pl.pallas_call(whole_step, out_shape=jax.ShapeDtypeStruct((share, width),...  181 us

profile of v2, /device:TPU:0, one launch (start us, length us, event | category | flops | bytes accessed | tf_op | source)
XLA Modules:
  0.0 185.4 jit_solution(10593073012384068320)
XLA Ops:
  0.0 1.5 copy.15.rope_ref
  1.5 0.5 multiply_cosine_fusion
  2.1 0.8 pad_maximum_fusion.table_ref
  2.9 180.7 %shard_map.118 = bf16[64,4096]{1,0:T(8,128)(2,1)} custom-call(bf16[256,768]{1,0:T(8,128)(2,1)} %query_ref.1, bf16[256,512]{1,0:T(8,128)(2,1)} %latent_ref.1, bf16[256,64]{1,0:T(8,128)(2,1)} %copy.15.rope_ref, f32[256,128]{1,0:T(8,128)} %pad_maximum_fusion.table_ref, f32[1,512]{1,0:T(1,128)} %bitcast.4, f32[1,512]{1,0:T(1,128)} %bitcast.5, ...), custom_call_target="tpu_custom_call" | custom-call | tf_op jit(solution)/shard_map/pallas_call | solution.py:973
  183.6 1.9 %copy.17 = bf16[64,4096]{1,0:T(8,128)(2,1)} copy(bf16[64,4096]{1,0:T(8,128)(2,1)} %shard_map.118) | data formatting | bytes 1048576
  (2 shorter events, 0.0 us)

commit v3 on v2

--- a/solution.py
+++ b/solution.py
@@ -299,11 +299,11 @@
 def whole_step(
     query_ref,
     latent_ref,
-    rope_ref,
-    table_ref,
+    inverse_ref,
     lat_gain_ref,
     out_gain_ref,
     ffn_gain_ref,
+    rope_hbm,
     resid_hbm,
     kv_hbm,
     out_hbm,
@@ -312,6 +312,7 @@
     down_hbm,
     result_ref,
     lat_mine,
+    rope_mine,
     lat_buf,
     query,
     resid,
@@ -341,6 +342,7 @@
     local_sem,
     lat_send,
     lat_recv,
+    lat_pass_send,
     lat_spread_send,
     lat_spread_recv,
     turn_send,
@@ -410,6 +412,14 @@
         return copy
 
     own_rows = pl.ds(pl.multiple_of(col * share, share), share)
+    rope_copy = local(rope_hbm.at[own_rows, :], rope_mine, 8)
+    barrier = pltpu.get_barrier_semaphore()
+    for step in range(1, ranks):
+        pl.semaphore_signal(
+            barrier, inc=1, device_id=((rank + step) % ranks, col), device_id_type=MESH
+        )
+    for flip in col_flips[1:]:
+        pl.semaphore_signal(barrier, inc=1, device_id=(rank, flip), device_id_type=MESH)
     kv_copy = local(kv_hbm, kv_w, 0)
     out_copy = local(out_hbm, out_w, 1)
     resid_copy = local(resid_hbm.at[own_rows, :], resid, 2)
@@ -419,22 +429,22 @@
         swapped = jnp.concatenate([values[:, half:], values[:, :half]], axis=1)
         return values * cosine + swapped * sine
 
+    def table(start, count):
+        shape = (count, ROPE)
+        place = (start + lax.broadcasted_iota(jnp.int32, shape, 0)).astype(jnp.float32)
+        angle = place * inverse_ref[...]
+        sine = jnp.sin(angle)
+        low = lax.broadcasted_iota(jnp.int32, shape, 1) < ROPE // 2
+        return jnp.cos(angle), jnp.where(low, -sine, sine)
+
     wide = latent_ref[own_rows, :].astype(jnp.float32)
     wide = wide * lax.rsqrt(jnp.mean(wide * wide, axis=1, keepdims=True) + EPSILON)
     lat_mine[:, :latent] = (wide * lat_gain_ref[...]).astype(jnp.bfloat16)
-    key_rope = turned(
-        rope_ref[own_rows, :].astype(jnp.float32), table_ref[own_rows, :ROPE],
-        table_ref[own_rows, ROPE:],
-    ).astype(jnp.bfloat16)
+    cosine, sine = table(rank * rows + col * share, share)
+    rope_copy.wait()
+    key_rope = turned(rope_mine[...].astype(jnp.float32), cosine, sine).astype(jnp.bfloat16)
     lat_mine[:, latent:] = jnp.concatenate([key_rope, jnp.zeros_like(key_rope)], axis=1)
 
-    barrier = pltpu.get_barrier_semaphore()
-    for step in range(1, ranks):
-        pl.semaphore_signal(
-            barrier, inc=1, device_id=((rank + step) % ranks, col), device_id_type=MESH
-        )
-    for flip in col_flips[1:]:
-        pl.semaphore_signal(barrier, inc=1, device_id=(rank, flip), device_id_type=MESH)
     pl.semaphore_wait(barrier, ranks - 1 + COLUMNS - 1)
 
     def lat_piece(source, column):
@@ -447,14 +457,20 @@
             tp=col_flips[flip],
         )
 
-    for step in range(1, ranks):
+    for step in range(1, LINE):
         send(
             remote(
                 lat_mine, lat_piece(rank, col), lat_send.at[step - 1], lat_recv.at[rank],
-                sp=(rank + step) % ranks,
+                sp=(rank + PAIR * step) % ranks,
             ),
-            rank + step < ranks,
-        )
+            z + step < LINE,
+        )
+    send(
+        remote(
+            lat_mine, lat_piece(rank, col), lat_send.at[LINE - 1], lat_recv.at[rank], sp=mate
+        ),
+        x == 0,
+    )
     lat_spread(rank, lat_mine, 2, 2).start()
     lat_spread(rank, lat_mine, 1, 1).start()
     lat_buf[rank, own_rows, :] = lat_mine[...]
@@ -510,17 +526,15 @@
 
     turn(0)
     turn(1)
-    pump(0, 0)
-    pump(1, 0)
-    pump_down(0)
+    own_pumps = []
     own_copies = [local(own_part(kind, z), region(kind, rank), 3 + kind) for kind in range(2)]
     own_copies.append(local(down_hbm, down.at[:, down_own], 5))
 
+    cosine, sine = table(rank * rows, rows)
     for head in range(heads):
         at = head * (NOPE + ROPE)
         rotary = turned(
-            query_ref[:, at + NOPE : at + NOPE + ROPE].astype(jnp.float32), table_ref[:, :ROPE],
-            table_ref[:, ROPE:],
+            query_ref[:, at + NOPE : at + NOPE + ROPE].astype(jnp.float32), cosine, sine
         ).astype(jnp.bfloat16)
         query[head, :, :NOPE] = query_ref[:, at : at + NOPE]
         query[head, :, NOPE:] = jnp.concatenate([rotary, jnp.zeros_like(rotary)], axis=1)
@@ -530,15 +544,39 @@
     scale = math.log2(math.e) / math.sqrt(NOPE + ROPE)
     kv_copy.wait()
 
+    def lat_taken(source):
+        piece = lat_piece(source, col)
+        arrived(piece, lat_recv.at[source])
+        lat_spread(source, piece, 2, 2).start()
+        lat_spread(source, piece, 1, 1).start()
+
+    def lat_onward(place):
+        piece = lat_piece(place * PAIR + x, col)
+        return remote(
+            piece, piece, lat_pass_send.at[place], lat_recv.at[place * PAIR + x], sp=mate
+        )
+
+    for kind in range(2):
+        here = region(kind, rank)
+        own_pumps.append(
+            remote(
+                own_part(kind, z), here, pair_send.at[kind, 0], pair_recv.at[kind, 0], sp=mate
+            )
+        )
+    own_pumps.append(
+        remote(
+            down_hbm.at[down_part(0), :], down.at[down_part(0), down_own], down_send.at[0],
+            down_recv.at[0], sp=mate,
+        )
+    )
+    pending += [(copy, None) for copy in own_pumps]
+
     def attend(index, carry):
         source = rank - index
 
-        @pl.when(index < rank)
+        @pl.when((index < rank) & ((source - 1) % PAIR != x) & (index + x > 0))
         def _():
-            arrived(lat_piece(source - 1, col), lat_recv.at[source - 1])
-            piece = lat_piece(source - 1, col)
-            lat_spread(source - 1, piece, 2, 2).start()
-            lat_spread(source - 1, piece, 1, 1).start()
+            lat_taken(source - 1)
 
         arrived(lat_piece(source, col_flips[2]), lat_spread_recv.at[source, 1])
         lat_spread(source, lat_piece(source, col_flips[2]), 1, 3).start()
@@ -568,6 +606,23 @@
                 weights.astype(jnp.bfloat16), key_value[:, at + NOPE : at + NOPE + VDIM],
                 preferred_element_type=jnp.float32,
             )
+
+        @pl.when(index == 0)
+        def _():
+            def onward(step, carry):
+                lat_taken((z - 1 - step) * PAIR + x)
+                lat_onward(z - 1 - step).start()
+                return carry
+
+            lax.fori_loop(0, z, onward, 0)
+
+            @pl.when((x == 0) & (rank > 0))
+            def _():
+                lat_taken(rank - 1)
+
+            for copy in own_pumps:
+                copy.start()
+
         return carry
 
     lax.fori_loop(0, rank + 1, attend, 0)
@@ -935,6 +990,12 @@
 
     lax.fori_loop(0, rank + 1, drain, 0)
 
+    def drain_onward(place, carry):
+        lat_onward(place).wait_send()
+        return carry
+
+    lax.fori_loop(0, z, drain_onward, 0)
+
 
 def fused_body(
     resid,
@@ -951,19 +1012,15 @@
     down_weight,
 ):
     ranks, columns = lax.axis_size("sp"), lax.axis_size("tp")
-    rank = lax.axis_index("sp")
     rows, width = resid.shape
     share = rows // columns
     heads = queries.shape[1] // (NOPE + ROPE)
     units = gate_weight.shape[1] // LINE
     block = gate_weight.shape[0]
     depth = latent.shape[1]
-    places = (rank * rows + jnp.arange(rows, dtype=jnp.int32)).astype(jnp.float32)
     half = ROPE // 2
     inverse = THETA ** (-jnp.arange(half, dtype=jnp.float32) / half)
-    angle = places[:, None] * inverse
-    cosine, sine = jnp.cos(angle), jnp.sin(angle)
-    table = jnp.concatenate([cosine, cosine, -sine, sine], axis=1)
+    inverse = jnp.concatenate([inverse, inverse]).reshape(1, ROPE)
     bf, f32 = jnp.bfloat16, jnp.float32
     dma = pltpu.SemaphoreType.DMA
     vmem = pl.BlockSpec(memory_space=pltpu.VMEM)
@@ -973,10 +1030,11 @@
     return pl.pallas_call(
         whole_step,
         out_shape=jax.ShapeDtypeStruct((share, width), bf),
-        in_specs=[vmem] * 7 + [anywhere] * 6,
+        in_specs=[vmem] * 6 + [anywhere] * 7,
         out_specs=vmem,
         scratch_shapes=[
             pltpu.VMEM((share, depth + LANES), bf),
+            pltpu.VMEM((share, ROPE), bf),
             pltpu.VMEM((ranks, rows, depth + LANES), bf),
             pltpu.VMEM((heads, rows, 2 * LANES), bf),
             pltpu.VMEM((share, width), bf),
@@ -1003,9 +1061,10 @@
             pltpu.VMEM((LINE, share, part), bf),
             pltpu.VMEM((share, width), bf),
             pltpu.VMEM((share, width), f32),
-            dma((6,)),
-            dma((ranks - 1,)),
+            dma((9,)),
+            dma((LINE,)),
             dma((ranks,)),
+            dma((LINE,)),
             dma((ranks, others)),
             dma((ranks, others)),
             dma((2, LINE)),
@@ -1040,11 +1099,11 @@
     )(
         queries,
         latent,
-        rope_key,
-        table,
+        inverse,
         lat_gain.reshape(1, -1),
         out_gain.reshape(1, -1),
         ffn_gain.reshape(1, -1),
+        rope_key,
         resid,
         kv_weight,
         out_weight,

time: 189 us -> 181 us (0.958)
  the two profiles are of different devices: /device:TPU:0 before, /device:TPU:17 now
where the time goes in v3:
time: 181 us
  Pallas kernels  177 us (98%)
  local copies, waits for them, and re-layouts  3.36 us (2%)
    pallas_call x1, Pallas kernels, fused_body(): pl.pallas_call(whole_step, out_shape=jax.ShapeDtypeStruct((share, width),...  177 us

profile of v3, /device:TPU:17, one launch (start us, length us, event | category | flops | bytes accessed | tf_op | source)
XLA Modules:
  0.0 180.8 jit_solution(59502272358831617)
XLA Ops:
  0.0 0.7 maximum_bitcast_fusion.inverse_ref
  0.7 1.5 copy.13.rope_hbm
  2.2 176.8 %shard_map.118 = bf16[64,4096]{1,0:T(8,128)(2,1)} custom-call(bf16[256,768]{1,0:T(8,128)(2,1)} %query_ref.1, bf16[256,512]{1,0:T(8,128)(2,1)} %latent_ref.1, f32[1,64]{1,0:T(1,128)} %maximum_bitcast_fusion.inverse_ref, f32[1,512]{1,0:T(1,128)} %bitcast.6, f32[1,512]{1,0:T(1,128)} %bitcast.7, f32[1,4096]{1,0:T(1,128)} %bitcast.5, ...), custom_call_target="tpu_custom_call" | custom-call | tf_op jit(solution)/shard_map/pallas_call | solution.py:1030
  179.0 1.9 %copy.15 = bf16[64,4096]{1,0:T(8,128)(2,1)} copy(bf16[64,4096]{1,0:T(8,128)(2,1)} %shard_map.118) | data formatting | bytes 1048576
  (1 shorter events, 0.0 us)

commit v4 on v3

--- a/solution.py
+++ b/solution.py
@@ -3,6 +3,7 @@
 
 import jax
 import jax.numpy as jnp
+import numpy as np
 from jax import lax
 from jax.experimental import pallas as pl
 from jax.experimental.pallas import tpu as pltpu
@@ -297,12 +298,12 @@
 
 
 def whole_step(
-    query_ref,
-    latent_ref,
     inverse_ref,
     lat_gain_ref,
     out_gain_ref,
     ffn_gain_ref,
+    query_hbm,
+    latent_hbm,
     rope_hbm,
     resid_hbm,
     kv_hbm,
@@ -313,6 +314,9 @@
     result_ref,
     lat_mine,
     rope_mine,
+    rope_wide,
+    wide_mine,
+    query_ref,
     lat_buf,
     query,
     resid,
@@ -412,7 +416,8 @@
         return copy
 
     own_rows = pl.ds(pl.multiple_of(col * share, share), share)
-    rope_copy = local(rope_hbm.at[own_rows, :], rope_mine, 8)
+    wide_copy = local(latent_hbm.at[own_rows, :], wide_mine, 9)
+    rope_copy = local(rope_hbm, rope_mine, 8)
     barrier = pltpu.get_barrier_semaphore()
     for step in range(1, ranks):
         pl.semaphore_signal(
@@ -420,6 +425,7 @@
         )
     for flip in col_flips[1:]:
         pl.semaphore_signal(barrier, inc=1, device_id=(rank, flip), device_id_type=MESH)
+    query_copy = local(query_hbm, query_ref, 10)
     kv_copy = local(kv_hbm, kv_w, 0)
     out_copy = local(out_hbm, out_w, 1)
     resid_copy = local(resid_hbm.at[own_rows, :], resid, 2)
@@ -437,12 +443,14 @@
         low = lax.broadcasted_iota(jnp.int32, shape, 1) < ROPE // 2
         return jnp.cos(angle), jnp.where(low, -sine, sine)
 
-    wide = latent_ref[own_rows, :].astype(jnp.float32)
+    cosine, sine = table(rank * rows + col * share, share)
+    wide_copy.wait()
+    wide = wide_mine[...].astype(jnp.float32)
     wide = wide * lax.rsqrt(jnp.mean(wide * wide, axis=1, keepdims=True) + EPSILON)
     lat_mine[:, :latent] = (wide * lat_gain_ref[...]).astype(jnp.bfloat16)
-    cosine, sine = table(rank * rows + col * share, share)
     rope_copy.wait()
-    key_rope = turned(rope_mine[...].astype(jnp.float32), cosine, sine).astype(jnp.bfloat16)
+    rope_wide[...] = jnp.transpose(rope_mine[...].astype(jnp.float32))
+    key_rope = turned(rope_wide[own_rows, :], cosine, sine).astype(jnp.bfloat16)
     lat_mine[:, latent:] = jnp.concatenate([key_rope, jnp.zeros_like(key_rope)], axis=1)
 
     pl.semaphore_wait(barrier, ranks - 1 + COLUMNS - 1)
@@ -531,6 +539,7 @@
     own_copies.append(local(down_hbm, down.at[:, down_own], 5))
 
     cosine, sine = table(rank * rows, rows)
+    query_copy.wait()
     for head in range(heads):
         at = head * (NOPE + ROPE)
         rotary = turned(
@@ -1019,8 +1028,8 @@
     block = gate_weight.shape[0]
     depth = latent.shape[1]
     half = ROPE // 2
-    inverse = THETA ** (-jnp.arange(half, dtype=jnp.float32) / half)
-    inverse = jnp.concatenate([inverse, inverse]).reshape(1, ROPE)
+    inverse = np.power(np.float32(THETA), -np.arange(half, dtype=np.float32) / np.float32(half))
+    inverse = jnp.asarray(np.concatenate([inverse, inverse]).reshape(1, ROPE), jnp.float32)
     bf, f32 = jnp.bfloat16, jnp.float32
     dma = pltpu.SemaphoreType.DMA
     vmem = pl.BlockSpec(memory_space=pltpu.VMEM)
@@ -1030,11 +1039,14 @@
     return pl.pallas_call(
         whole_step,
         out_shape=jax.ShapeDtypeStruct((share, width), bf),
-        in_specs=[vmem] * 6 + [anywhere] * 7,
+        in_specs=[vmem] * 4 + [anywhere] * 9,
         out_specs=vmem,
         scratch_shapes=[
             pltpu.VMEM((share, depth + LANES), bf),
-            pltpu.VMEM((share, ROPE), bf),
+            pltpu.VMEM((ROPE, rows), bf),
+            pltpu.VMEM((rows, ROPE), f32),
+            pltpu.VMEM((share, depth), bf),
+            pltpu.VMEM(queries.shape, bf),
             pltpu.VMEM((ranks, rows, depth + LANES), bf),
             pltpu.VMEM((heads, rows, 2 * LANES), bf),
             pltpu.VMEM((share, width), bf),
@@ -1061,7 +1073,7 @@
             pltpu.VMEM((LINE, share, part), bf),
             pltpu.VMEM((share, width), bf),
             pltpu.VMEM((share, width), f32),
-            dma((9,)),
+            dma((11,)),
             dma((LINE,)),
             dma((ranks,)),
             dma((LINE,)),
@@ -1097,13 +1109,13 @@
             collective_id=0, has_side_effects=True, vmem_limit_bytes=66 * 1024 * 1000
         ),
     )(
-        queries,
-        latent,
         inverse,
         lat_gain.reshape(1, -1),
         out_gain.reshape(1, -1),
         ffn_gain.reshape(1, -1),
-        rope_key,
+        queries,
+        latent,
+        rope_key.T,
         resid,
         kv_weight,
         out_weight,

time: 181 us -> 179 us (0.989)
  no operation moved by 1% of the time
where the time goes in v4:
time: 179 us; the launch traced here: 178 us
  Pallas kernels  176 us (98%)
  local copies, waits for them, and re-layouts  1.87 us (1%)
    pallas_call x1, Pallas kernels, fused_body(): pl.pallas_call(whole_step, out_shape=jax.ShapeDtypeStruct((share, width),...  176 us

profile of v4, /device:TPU:17, one launch (start us, length us, event | category | flops | bytes accessed | tf_op | source)
XLA Modules:
  0.0 178.3 jit_solution(12426302714131777992)
XLA Ops:
  0.0 176.5 %shard_map.127 = bf16[64,4096]{1,0:T(8,128)(2,1)} custom-call(f32[1,64]{1,0:T(1,128)} %constant.2.clone.inverse_ref, f32[1,512]{1,0:T(1,128)} %bitcast.6, f32[1,512]{1,0:T(1,128)} %bitcast.7, f32[1,4096]{1,0:T(1,128)} %bitcast.5, bf16[256,768]{1,0:T(8,128)(2,1)} %query_hbm.1, bf16[256,512]{1,0:T(8,128)(2,1)} %latent_hbm.1, bf16[64,256]{1,0:T(8,128)(2,1)} %bitcast.4, ...), custom_call_target="tpu_custom_call" | custom-call | tf_op jit(solution)/shard_map/pallas_call | solution.py:1039
  176.5 1.9 %copy.15 = bf16[64,4096]{1,0:T(8,128)(2,1)} copy(bf16[64,4096]{1,0:T(8,128)(2,1)} %shard_map.127) | data formatting | bytes 1048576
